TPU v7x, 32 devices: a whole 2x2x4 slice. The times are simulated.
32 devices in a mesh: ep: 8 (over z, x), tp: 4 (over y, core).
Axes of the slice: x: 2, y: 2, z: 4, core: 2. Of those that a mesh axis runs over, the one named last changes fastest.
Arguments:
- tokens: bfloat16 [1024, 2048], P('ep'), may hold values from -6 to 6
- routing: int32 [1024, 2], P('ep'), may hold values from 0 to 7, all different within a row; in each aligned block of 128 rows (0 to 127, 128 to 255, ...) at most 56 rows name the same one
- router_weight: bfloat16 [2048, 8], replicated, may hold values from -0.125 to 0.125
- gate_weight: bfloat16 [8, 2048, 2048], P('ep', None, 'tp'), may hold values from -0.125 to 0.125
- up_weight: bfloat16 [8, 2048, 2048], P('ep', None, 'tp'), may hold values from -0.125 to 0.125
- down_weight: bfloat16 [8, 2048, 2048], P('ep', 'tp'), may hold values from -0.125 to 0.125
- cotangent: bfloat16 [1024, 2048], P('ep'), may hold values from -0.796875 to 0.796875
Outputs:
- token_grad: bfloat16 [1024, 2048], P('ep')
- router_grad: float32 [2048, 8], P('tp')
- router_rows: float32 [2048], P('tp')
- gate_grad: bfloat16 [8, 2048, 2048], P('ep', None, 'tp')
- up_grad: bfloat16 [8, 2048, 2048], P('ep', None, 'tp')
- down_grad: bfloat16 [8, 2048, 2048], P('ep', 'tp')
- gate_rows: float32 [8, 2048], P('ep')
- up_rows: float32 [8, 2048], P('ep')
- down_rows: float32 [8, 2048], P('ep', 'tp')
Inputs may be any that keep to these rules, and one draw needn't show every extreme that they name: `routing`: A row's 2 experts differ. Within the rows of one index of ep (128 rows), no expert is named more than 56 times, a bound that some block reaches.
All inputs are finite; a program needn't handle non-finite values.
Results may differ from a plain program's by a relative error of at most 0.01.
Values may be sent and summed in bfloat16 or wider, within the bound.
A program may use at most 64 MiB of HBM per device.

v0:
```python
import jax
import jax.numpy as jnp
from jax import lax
from jax.sharding import PartitionSpec as P


def expert_backward(rows_in, cots_in, slot_scale, w_gate, w_up, w_down):
    pre_gate = jnp.dot(rows_in, w_gate, preferred_element_type=jnp.float32)
    pre_up = jnp.dot(rows_in, w_up, preferred_element_type=jnp.float32)
    sigmoid_gate = jax.nn.sigmoid(pre_gate)
    hidden = (pre_gate * sigmoid_gate * pre_up).astype(jnp.bfloat16)
    back_proj = lax.dot_general(
        cots_in, w_down, (((1,), (1,)), ((), ())), preferred_element_type=jnp.float32
    )
    gate_term = jnp.sum(hidden.astype(jnp.float32) * back_proj, axis=1)
    scaled = slot_scale * back_proj
    grad_up_pre = (scaled * pre_gate * sigmoid_gate).astype(jnp.bfloat16)
    grad_gate_pre = (
        scaled * pre_up * sigmoid_gate * (1.0 + pre_gate * (1.0 - sigmoid_gate))
    ).astype(jnp.bfloat16)
    weighted = (slot_scale * cots_in.astype(jnp.float32)).astype(jnp.bfloat16)
    contract_rows = (((0,), (0,)), ((), ()))
    grad_down = lax.dot_general(hidden, weighted, contract_rows, preferred_element_type=jnp.float32)
    grad_gate = lax.dot_general(
        rows_in, grad_gate_pre, contract_rows, preferred_element_type=jnp.float32
    )
    grad_up = lax.dot_general(
        rows_in, grad_up_pre, contract_rows, preferred_element_type=jnp.float32
    )
    contract_hidden = (((1,), (1,)), ((), ()))
    partial_value = lax.dot_general(
        grad_gate_pre, w_gate, contract_hidden, preferred_element_type=jnp.float32
    )
    partial_value = partial_value + lax.dot_general(
        grad_up_pre, w_up, contract_hidden, preferred_element_type=jnp.float32
    )
    return (partial_value, gate_term, grad_gate, grad_up, grad_down)


def per_device(tokens, routing, router_weight, gate_weight, up_weight, down_weight, cotangent):
    groups = lax.axis_size("ep")
    shares = lax.axis_size("tp")
    tok_count, model_width = tokens.shape
    top_count = routing.shape[1]
    local_experts = gate_weight.shape[0]
    experts = local_experts * groups
    capacity = 7 * tok_count * top_count // (4 * experts)
    slot_span = groups * capacity
    assigns = tok_count * top_count
    col_width = model_width // shares
    col_start = lax.axis_index("tp") * col_width
    logits = jnp.dot(tokens, router_weight, preferred_element_type=jnp.float32)
    affinity = jax.nn.sigmoid(logits)
    chosen = jnp.take_along_axis(affinity, routing, axis=1)
    total_aff = jnp.sum(chosen, axis=1, keepdims=True)
    weights = chosen / total_aff
    flat_ids = routing.reshape(-1)
    onehot_ids = (flat_ids[:, None] == jnp.arange(experts, dtype=jnp.int32)[None, :]).astype(
        jnp.int32
    )
    position = jnp.sum((jnp.cumsum(onehot_ids, axis=0) - 1) * onehot_ids, axis=1)
    slot_of = flat_ids % local_experts * slot_span + flat_ids // local_experts * capacity + position
    slot_table = jnp.full((local_experts * slot_span,), assigns, jnp.int32)
    slot_table = slot_table.at[slot_of].set(jnp.arange(assigns, dtype=jnp.int32))
    zero_row = jnp.zeros((1, model_width), jnp.bfloat16)
    tok_pad = jnp.concatenate([tokens, zero_row], axis=0)
    cot_pad = jnp.concatenate([cotangent, zero_row], axis=0)
    weight_pad = jnp.concatenate(
        [weights.astype(jnp.bfloat16).reshape(-1), jnp.zeros((1,), jnp.bfloat16)]
    )
    source_tok = slot_table // top_count
    rows_send = tok_pad[source_tok].reshape(local_experts, groups, capacity, model_width)
    cots_send = cot_pad[source_tok].reshape(local_experts, groups, capacity, model_width)
    scale_send = weight_pad[slot_table].reshape(local_experts, groups, capacity)
    rows_recv, cots_recv, scale_recv = (
        lax.all_to_all(rows_send, "ep", split_axis=1, concat_axis=1, tiled=True),
        lax.all_to_all(cots_send, "ep", split_axis=1, concat_axis=1, tiled=True),
        lax.all_to_all(scale_send, "ep", split_axis=1, concat_axis=1, tiled=True),
    )
    partials, gate_terms, gate_grads, up_grads, down_grads = ([], [], [], [], [])
    slot_scale = scale_recv[0].reshape(slot_span).astype(jnp.float32)[:, None]
    result = expert_backward(
        rows_recv[0].reshape(slot_span, model_width),
        cots_recv[0].reshape(slot_span, model_width),
        slot_scale,
        gate_weight[0],
        up_weight[0],
        down_weight[0],
    )
    partials.append(result[0])
    gate_terms.append(result[1])
    gate_grads.append(result[2])
    up_grads.append(result[3])
    down_grads.append(result[4])
    partial_value = jnp.stack(partials)
    gate_term = jnp.stack(gate_terms)
    grad_gate = jnp.stack(gate_grads)
    grad_up = jnp.stack(up_grads)
    grad_down = jnp.stack(down_grads)
    gate_rows, up_rows = lax.psum(
        (jnp.sum(grad_gate * grad_gate, axis=2), jnp.sum(grad_up * grad_up, axis=2)), "tp"
    )
    down_rows = jnp.sum(grad_down * grad_down, axis=2)
    summed = lax.psum_scatter(partial_value, "tp", scatter_dimension=2, tiled=True)
    gate_sum = lax.psum(gate_term, "tp")
    back_send = summed.astype(jnp.bfloat16).reshape(local_experts, groups, capacity, col_width)
    gate_send = gate_sum.astype(jnp.bfloat16).reshape(local_experts, groups, capacity)
    back_recv, gate_recv = (
        lax.all_to_all(back_send, "ep", split_axis=1, concat_axis=1, tiled=True),
        lax.all_to_all(gate_send, "ep", split_axis=1, concat_axis=1, tiled=True),
    )
    router_cols = lax.dynamic_slice_in_dim(router_weight, col_start, col_width, 0)
    back_flat = back_recv.reshape(local_experts * slot_span, -1)
    back_rows = jnp.sum(
        back_flat[slot_of].astype(jnp.float32).reshape(tok_count, top_count, -1), axis=1
    )
    d_weights = gate_recv.reshape(-1)[slot_of].astype(jnp.float32).reshape(tok_count, top_count)
    d_chosen = (d_weights - jnp.sum(d_weights * weights, axis=1, keepdims=True)) / total_aff
    d_logit = d_chosen * chosen * (1.0 - chosen)
    onehot = (routing[:, :, None] == jnp.arange(experts, dtype=jnp.int32)[None, None, :]).astype(
        jnp.float32
    )
    d_logits = jnp.sum(d_logit[:, :, None] * onehot, axis=1).astype(jnp.bfloat16)
    token_cols = lax.dynamic_slice_in_dim(tokens, col_start, col_width, 1)
    router_part = lax.dot_general(
        token_cols, d_logits, (((0,), (0,)), ((), ())), preferred_element_type=jnp.float32
    )
    router_grad = lax.psum(router_part, "ep")
    router_rows = jnp.sum(router_grad * router_grad, axis=1)
    router_back = lax.dot_general(
        d_logits, router_cols, (((1,), (1,)), ((), ())), preferred_element_type=jnp.float32
    )
    token_grad = (back_rows + router_back).astype(jnp.bfloat16)
    token_grad = lax.all_gather(token_grad, "tp", axis=1, tiled=True)
    return (
        token_grad,
        router_grad,
        router_rows,
        grad_gate.astype(jnp.bfloat16),
        grad_up.astype(jnp.bfloat16),
        grad_down.astype(jnp.bfloat16),
        gate_rows,
        up_rows,
        down_rows,
    )


def solution(mesh):
    return jax.shard_map(
        per_device,
        mesh=mesh,
        in_specs=(
            P("ep", None),
            P("ep", None),
            P(),
            P("ep", None, "tp"),
            P("ep", None, "tp"),
            P("ep", "tp", None),
            P("ep", None),
        ),
        out_specs=(
            P("ep", None),
            P("tp", None),
            P("tp"),
            P("ep", None, "tp"),
            P("ep", None, "tp"),
            P("ep", "tp", None),
            P("ep", None),
            P("ep", None),
            P("ep", "tp"),
        ),
        check_vma=False,
    )
```

profile of v0, /device:TPU:0, one launch (start us, length us, event | category | flops | bytes accessed | tf_op | source)
XLA Modules:
  0.0 255.0 jit_solution(7731860463774829727)
XLA Ops:
  7.2 0.8 broadcast_multiply_fusion
  8.0 0.8 copy.81
  8.8 0.1 eq.44
  8.9 0.1 eq.40
  9.1 0.7 bitcast_or_fusion
  9.8 0.1 copy.80
  9.9 0.1 mul.106
  10.0 0.6 reduce-window.6
  10.6 0.2 slice_reduce_fusion
  10.9 0.1 fusion.17
  11.0 1.4 scatter_custom_fusion
  12.4 0.1 copy.77
  12.6 0.1 reshape.207
  12.7 1.3 fusion.14
  14.0 1.4 gather_fusion.5
  15.4 0.1 reshape.210
  15.5 0.1 copy.78
  15.6 0.6 fusion.29
  16.2 0.1 copy.79
  16.4 0.1 convert_element_type.88
  16.6 3.2 %gather_fusion = bf16[448]{0:T(512)(128)(2,1)S(1)} fusion(bf16[257]{0:T(512)(128)(2,1)S(1)} %pad_maximum_fusion, s32[1024]{0:T(1024)S(1)} %get-tuple-element.83), kind=kCustom, calls=%fused_computation | custom fusion | bytes 3584 | tf_op jit(solution)/shard_map/gather | solution.py:74
  19.7 0.7 reshape.229
  20.4 7.3 %all-to-all-start = ((bf16[1,8,56]{2,0,1:T(2,128)(2,1)}), bf16[1,8,56]{2,0,1:T(2,128)(2,1)S(1)}, u32[]{:S(2)}, u32[]{:S(2)}) async-start(bf16[1,8,56]{2,0,1:T(2,128)(2,1)} %reshape.229), calls=%async_computation | async-start | bytes 8192 | tf_op jit(solution)/shard_map/all_to_all | solution.py:78
  27.7 3.2 %gather_fusion.2 = bf16[448,2048]{1,0:T(8,128)(2,1)} fusion(bf16[129,2048]{1,0:T(8,128)(2,1)S(1)} %concatenate.11, s32[1024]{0:T(1024)S(1)} %get-tuple-element.82), kind=kCustom, calls=%fused_computation.2 | custom fusion | bytes 3671808 | tf_op jit(solution)/shard_map/gather | solution.py:72
  30.9 3.2 %all-to-all-done = bf16[1,8,56]{2,0,1:T(2,128)(2,1)S(1)} async-done(((bf16[1,8,56]{2,0,1:T(2,128)(2,1)}), bf16[1,8,56]{2,0,1:T(2,128)(2,1)S(1)}, u32[]{:S(2)}, u32[]{:S(2)}) %all-to-all-start) | async-done | bytes 928 | tf_op jit(solution)/shard_map/all_to_all | solution.py:78
  34.1 4.3 %all-to-all-start.2 = ((bf16[1,8,56,2048]{3,2,0,1:T(8,128)(2,1)}), bf16[1,8,56,2048]{3,2,0,1:T(8,128)(2,1)}, u32[]{:S(2)}, u32[]{:S(2)}) async-start(bf16[1,8,56,2048]{3,2,0,1:T(8,128)(2,1)} %bitcast.67), calls=%async_computation.2 | async-start | bytes 3670016 | tf_op jit(solution)/shard_map/all_to_all | solution.py:76
  38.4 1.1 concatenate.10
  39.5 3.2 %gather_fusion.1 = bf16[448,2048]{1,0:T(8,128)(2,1)} fusion(bf16[129,2048]{1,0:T(8,128)(2,1)S(1)} %concatenate.10, s32[1024]{0:T(1024)S(1)} %get-tuple-element.82), kind=kCustom, calls=%fused_computation.1 | custom fusion | bytes 3671808 | tf_op jit(solution)/shard_map/gather | solution.py:73
  42.7 37.2 %all-to-all-done.2 = bf16[1,8,56,2048]{3,2,0,1:T(8,128)(2,1)} async-done(((bf16[1,8,56,2048]{3,2,0,1:T(8,128)(2,1)}), bf16[1,8,56,2048]{3,2,0,1:T(8,128)(2,1)}, u32[]{:S(2)}, u32[]{:S(2)}) %all-to-all-start.2) | async-done | bytes 1835040 | tf_op jit(solution)/shard_map/all_to_all | solution.py:76
  79.9 4.3 %all-to-all-start.1 = ((bf16[1,8,56,2048]{3,2,0,1:T(8,128)(2,1)}), bf16[1,8,56,2048]{3,2,0,1:T(8,128)(2,1)}, u32[]{:S(2)}, u32[]{:S(2)}) async-start(bf16[1,8,56,2048]{3,2,0,1:T(8,128)(2,1)} %bitcast.66), calls=%async_computation.1 | async-start | bytes 3670016 | tf_op jit(solution)/shard_map/all_to_all | solution.py:77
  84.2 0.2 reduce-scatter.2.cloned.1.call-start
  84.5 0.1 reshape.164
  84.6 4.2 %fusion.5 = f32[448,512]{1,0:T(8,128)} fusion(bf16[448,2048]{1,0:T(8,128)(2,1)} %bitcast.11, bf16[1,2048,512]{2,1,0:T(8,128)(2,1)} %param.11), kind=kOutput, calls=%fused_computation.17 | convolution fusion | flops 939524096 | bytes 4849664 | tf_op jit(solution)/shard_map/dot_general | solution.py:9
  88.8 3.5 %fusion.2 = f32[448,512]{1,0:T(8,128)} fusion(bf16[448,2048]{1,0:T(8,128)(2,1)} %bitcast.11, bf16[1,2048,512]{2,1,0:T(8,128)(2,1)S(1)} %copy-done), kind=kOutput, calls=%fused_computation.14 | convolution fusion | flops 939524096 | bytes 4849664 | tf_op jit(solution)/shard_map/dot_general | solution.py:8
  92.3 34.1 %all-to-all-done.1 = bf16[1,8,56,2048]{3,2,0,1:T(8,128)(2,1)} async-done(((bf16[1,8,56,2048]{3,2,0,1:T(8,128)(2,1)}), bf16[1,8,56,2048]{3,2,0,1:T(8,128)(2,1)}, u32[]{:S(2)}, u32[]{:S(2)}) %all-to-all-start.1) | async-done | bytes 1835040 | tf_op jit(solution)/shard_map/all_to_all | solution.py:77
  126.4 5.5 %multiply_reduce_fusion.3 = (f32[448]{0:T(512)}, bf16[448,512]{1,0:T(8,128)(2,1)}, bf16[448,512]{1,0:T(8,128)(2,1)S(1)}, bf16[448,512]{1,0:T(8,128)(2,1)S(1)}) fusion(f32[448,512]{1,0:T(8,128)} %fusion.5, f32[448,512]{1,0:T(8,128)} %fusion.2, f32[448]{0:T(512)S(1)} %reshape.164, bf16[448,2048]{1,0:T(8,128)(2,1)} %bitcast.7, bf16[1,512,2048]{2,1,0:T(8,128)(2,1)} %param.12), kind=kOutput, calls=%fused_computation.32 | convolution fusion | flops 944111168 | bytes 7147008 | tf_op jit(solution)/shard_map/dot_general | solution.py:12
  131.9 1.1 fusion
  133.1 0.4 copy-done.2
  133.5 3.0 %add_bitcast_fusion = f32[1,448,2048]{2,1,0:T(8,128)} fusion(f32[448,2048]{1,0:T(8,128)S(1)} %fusion, bf16[448,512]{1,0:T(8,128)(2,1)S(1)} %get-tuple-element.79, bf16[1,2048,512]{2,1,0:T(8,128)(2,1)S(1)} %copy-done.2), kind=kOutput, calls=%fused_computation.11 | convolution fusion | flops 940441600 | bytes 9895936 | tf_op jit(solution)/shard_map/dot_general | solution.py:34
  136.5 0.0 reduce-scatter.2.cloned.1.call-update
  136.6 4.1 %convert_bitcast_fusion.2 = (bf16[1,2048,512]{1,2,0:T(8,128)(2,1)}, f32[2048]{0:T(1024)S(1)}) fusion(bf16[448,2048]{1,0:T(8,128)(2,1)} %bitcast.11, bf16[448,512]{1,0:T(8,128)(2,1)S(1)} %get-tuple-element.78), kind=kOutput, calls=%fused_computation.23 | convolution fusion | flops 942667776 | bytes 4399104 | tf_op jit(solution)/shard_map/dot_general | solution.py:24
  140.7 4.3 %convert_bitcast_fusion.1 = (bf16[1,2048,512]{1,2,0:T(8,128)(2,1)}, f32[2048]{0:T(1024)S(1)}) fusion(bf16[448,2048]{1,0:T(8,128)(2,1)} %bitcast.11, bf16[448,512]{1,0:T(8,128)(2,1)S(1)} %get-tuple-element.79), kind=kOutput, calls=%fused_computation.22 | convolution fusion | flops 942667776 | bytes 4399104 | tf_op jit(solution)/shard_map/dot_general | solution.py:27
  145.0 11.0 %all-reduce.2 = (bf16[1,448]{1,0:T(2,128)(2,1)S(1)}, f32[1,2048]{1,0:T(1,128)}, f32[1,2048]{1,0:T(1,128)}) all-reduce(f32[1,448]{1,0:T(1,128)S(1)} %bitcast.73, f32[1,2048]{1,0:T(1,128)S(1)} %bitcast.68, f32[1,2048]{1,0:T(1,128)S(1)} %bitcast.69), channel_id=1, replica_groups=mesh['ep'=8,'tp'=4] {'tp'}, use_global_device_ids=true, to_apply=%region_8.9 | all-reduce | flops 4544 | bytes 35456 | tf_op jit(solution)/shard_map/psum | solution.py:105
  156.0 0.7 reshape.230
  156.7 4.5 %all-to-all-start.4 = ((bf16[1,8,56]{2,0,1:T(2,128)(2,1)}), bf16[1,8,56]{2,0,1:T(2,128)(2,1)S(1)}, u32[]{:S(2)}, u32[]{:S(2)}) async-start(bf16[1,8,56]{2,0,1:T(2,128)(2,1)} %reshape.230), calls=%async_computation.5 | async-start | bytes 8192 | tf_op jit(solution)/shard_map/all_to_all | solution.py:110
  161.3 15.6 %reduce-scatter.2.cloned.1.call-done = f32[1,448,512]{2,1,0:T(8,128)} async-done(((f32[1,448,2048]{2,1,0:T(8,128)}), f32[1,448,512]{2,1,0:T(8,128)}) %reduce-scatter.2.cloned.1.call-update) | async-done | bytes 917520 | tf_op jit(solution)/shard_map/reduce_scatter | solution.py:104
  176.9 2.0 convert_element_type.94
  178.9 5.5 %all-to-all-start.3 = ((bf16[1,8,56,512]{3,2,0,1:T(8,128)(2,1)}), bf16[1,8,56,512]{3,2,0,1:T(8,128)(2,1)S(1)}, u32[]{:S(2)}, u32[]{:S(2)}) async-start(bf16[1,8,56,512]{3,2,0,1:T(8,128)(2,1)} %bitcast.16), calls=%async_computation.4 | async-start | bytes 917504 | tf_op jit(solution)/shard_map/all_to_all | solution.py:109
  184.4 4.9 %multiply_reduce_fusion = (f32[512]{0:T(512)}, bf16[1,512,2048]{2,1,0:T(8,128)(2,1)}) fusion(bf16[448,512]{1,0:T(8,128)(2,1)} %get-tuple-element.67, bf16[448,2048]{1,0:T(8,128)(2,1)} %bitcast.7, f32[448]{0:T(512)S(1)} %copy-done.11), kind=kOutput, calls=%fused_computation.7 | convolution fusion | flops 945421824 | bytes 4394752 | tf_op jit(solution)/shard_map/dot_general | solution.py:23
  189.3 3.9 %copy.90 = bf16[1,2048,512]{2,1,0:T(8,128)(2,1)} copy(bf16[1,2048,512]{1,2,0:T(8,128)(2,1)} %get-tuple-element.76) | data formatting | bytes 4194304
  193.3 3.9 %copy.91 = bf16[1,2048,512]{2,1,0:T(8,128)(2,1)} copy(bf16[1,2048,512]{1,2,0:T(8,128)(2,1)} %get-tuple-element.74) | data formatting | bytes 4194304
  197.2 0.1 reshape.163
  197.3 1.9 gather_fusion.4
  199.2 0.1 reshape.166
  199.4 0.1 copy.89
  199.5 0.1 fusion.15
  199.7 37.5 %psum.29 = f32[512,8]{0,1:T(8,128)S(1)} all-reduce(f32[512,8]{0,1:T(8,128)S(1)} %fusion.15), channel_id=1, replica_groups=mesh['ep'=8,'tp'=4] {'ep'}, use_global_device_ids=true, to_apply=%region_11.12 | all-reduce | flops 4096 | bytes 32768 | tf_op jit(solution)/shard_map/psum | solution.py:128
  237.2 0.6 multiply_reduce_fusion.4
  237.8 1.2 gather_fusion.3
  239.0 0.3 reshape.165
  239.3 0.6 reduce_sum.101
  239.9 0.9 fusion.11
  240.9 6.5 %all_gather.3 = bf16[128,2048]{1,0:T(8,128)(2,1)S(1)} all-gather(bf16[128,512]{1,0:T(8,128)(2,1)S(1)} %fusion.11), channel_id=1, replica_groups=mesh['ep'=8,'tp'=4] {'tp'}, dimensions={1}, use_global_device_ids=true | all-gather | bytes 655360 | tf_op jit(solution)/shard_map/all_gather | solution.py:134
  247.4 0.8 copy.93
  (44 shorter events, 0.4 us)
Async XLA Ops:
  7.2 81.6 %copy-start = (bf16[1,2048,512]{2,1,0:T(8,128)(2,1)S(1)}, bf16[1,2048,512]{2,1,0:T(8,128)(2,1)}, u32[]{:S(2)}) copy-start(bf16[1,2048,512]{2,1,0:T(8,128)(2,1)} %param.10) | copy-start | bytes 6291460
  11.0 1.7 copy-start.7
  14.0 1.6 copy-start.4
  14.0 13.7 %copy-start.1 = (bf16[128,2048]{1,0:T(8,128)(2,1)S(1)}, bf16[128,2048]{1,0:T(8,128)(2,1)}, u32[]{:S(2)}) copy-start(bf16[128,2048]{1,0:T(8,128)(2,1)} %param.7) | copy-start | bytes 1572868
  15.6 15.3 %copy-start.5 = (f32[128]{0:T(128)}, f32[128]{0:T(128)S(1)}, u32[]{:S(2)}) copy-start(f32[128]{0:T(128)S(1)} %get-tuple-element.70) | copy-start | bytes 1540
  20.4 13.7 %all-to-all-start = ((bf16[1,8,56]{2,0,1:T(2,128)(2,1)}), bf16[1,8,56]{2,0,1:T(2,128)(2,1)S(1)}, u32[]{:S(2)}, u32[]{:S(2)}) async-start(bf16[1,8,56]{2,0,1:T(2,128)(2,1)} %reshape.229), calls=%async_computation | async-start | bytes 8192 | tf_op jit(solution)/shard_map/all_to_all | solution.py:78
  34.1 45.8 %all-to-all-start.2 = ((bf16[1,8,56,2048]{3,2,0,1:T(8,128)(2,1)}), bf16[1,8,56,2048]{3,2,0,1:T(8,128)(2,1)}, u32[]{:S(2)}, u32[]{:S(2)}) async-start(bf16[1,8,56,2048]{3,2,0,1:T(8,128)(2,1)} %bitcast.67), calls=%async_computation.2 | async-start | bytes 3670016 | tf_op jit(solution)/shard_map/all_to_all | solution.py:76
  79.9 46.5 %all-to-all-start.1 = ((bf16[1,8,56,2048]{3,2,0,1:T(8,128)(2,1)}), bf16[1,8,56,2048]{3,2,0,1:T(8,128)(2,1)}, u32[]{:S(2)}, u32[]{:S(2)}) async-start(bf16[1,8,56,2048]{3,2,0,1:T(8,128)(2,1)} %bitcast.66), calls=%async_computation.1 | async-start | bytes 3670016 | tf_op jit(solution)/shard_map/all_to_all | solution.py:77
  84.2 92.7 %reduce-scatter.2.cloned.1.call-start = ((), (), s32[]{:S(2)}) async-start(), calls=%async_computation.6 | async-start | bytes 4587520 | tf_op jit(solution)/shard_map/reduce_scatter | solution.py:104
  84.6 41.8 %copy-start.10 = (f32[448]{0:T(512)}, f32[448]{0:T(512)S(1)}, u32[]{:S(2)}) copy-start(f32[448]{0:T(512)S(1)} %reshape.164) | copy-start | bytes 5380
  131.9 1.6 copy-start.2
  140.7 4.3 %copy-start.12 = (f32[448]{0:T(512)S(1)}, f32[448]{0:T(512)}, u32[]{:S(2)}) copy-start(f32[448]{0:T(512)} %get-tuple-element.66) | copy-start | bytes 5380
  140.7 20.6 %copy-start.8 = (s32[256,1]{0,1:T(1,128)S(1)}, s32[256,1]{0,1:T(1,128)}, u32[]{:S(2)}) copy-start(s32[256,1]{0,1:T(1,128)} %copy-done.7) | copy-start | bytes 3076
  145.0 39.4 %copy-start.11 = (f32[448]{0:T(512)S(1)}, f32[448]{0:T(512)}, u32[]{:S(2)}) copy-start(f32[448]{0:T(512)} %copy-done.10) | copy-start | bytes 5380
  156.7 22.2 %all-to-all-start.4 = ((bf16[1,8,56]{2,0,1:T(2,128)(2,1)}), bf16[1,8,56]{2,0,1:T(2,128)(2,1)S(1)}, u32[]{:S(2)}, u32[]{:S(2)}) async-start(bf16[1,8,56]{2,0,1:T(2,128)(2,1)} %reshape.230), calls=%async_computation.5 | async-start | bytes 8192 | tf_op jit(solution)/shard_map/all_to_all | solution.py:110
  178.9 58.9 %all-to-all-start.3 = ((bf16[1,8,56,512]{3,2,0,1:T(8,128)(2,1)}), bf16[1,8,56,512]{3,2,0,1:T(8,128)(2,1)S(1)}, u32[]{:S(2)}, u32[]{:S(2)}) async-start(bf16[1,8,56,512]{3,2,0,1:T(8,128)(2,1)} %bitcast.16), calls=%async_computation.4 | async-start | bytes 917504 | tf_op jit(solution)/shard_map/all_to_all | solution.py:109
  193.3 6.2 %copy-start.9 = (f32[128,2]{0,1:T(2,128)S(1)}, f32[128,2]{0,1:T(2,128)}, u32[]{:S(2)}) copy-start(f32[128,2]{0,1:T(2,128)} %get-tuple-element.69) | copy-start | bytes 3076
  193.3 6.2 %copy-start.6 = (f32[128]{0:T(128)S(1)}, f32[128]{0:T(128)}, u32[]{:S(2)}) copy-start(f32[128]{0:T(128)} %copy-done.5) | copy-start | bytes 1540
  237.2 3.7 %copy-start.3 = (f32[512,8]{0,1:T(8,128)}, f32[512,8]{0,1:T(8,128)S(1)}, u32[]{:S(2)}) copy-start(f32[512,8]{0,1:T(8,128)S(1)} %psum.29) | copy-start | bytes 49156
Sparse Core Ops, SparseCore 0:
  136.7 40.1 reduce-scatter.1
where the time goes:
time: 256 us; the launch traced here: 255 us
  waiting for transfers between devices  90.1 us (35%)
  blocking collectives  55 us (21%)
  matrix products  33.1 us (13%)
  local copies, waits for them, and re-layouts  30 us (12%)
  starting transfers between devices  26.2 us (10%)
  between operations  14.3 us (6%)
  other arithmetic  6.23 us (2%)
    psum x1, blocking collectives, per_device(): router_grad = lax.psum(router_part, 'ep')  37.5 us
    all_to_all x1, waiting for transfers between devices, per_device(): lax.all_to_all(rows_send, 'ep', split_axis=1, concat_axis=1, tiled=True)  37.2 us
    all_to_all x1, waiting for transfers between devices, per_device(): lax.all_to_all(cots_send, 'ep', split_axis=1, concat_axis=1, tiled=True)  34.1 us
    reduce_scatter x1, waiting for transfers between devices, per_device(): lax.psum_scatter(partial_value, 'tp', scatter_dimension=2, tiled=True)  15.6 us
    psum x1, blocking collectives, per_device(): gate_sum = lax.psum(gate_term, 'tp')  11 us
    unnamed x30, local copies, waits for them, and re-layouts  9.92 us
    all_to_all x1, starting transfers between devices, per_device(): lax.all_to_all(scale_send, 'ep', split_axis=1, concat_axis=1, tiled=True)  7.28 us
    all_gather x1, blocking collectives, per_device(): token_grad = lax.all_gather(token_grad, 'tp', axis=1, tiled=True)  6.5 us
  transfers between devices with their start and end apart: 6, of which 4 were waited for; matrix products, arithmetic and copies ran while one was open for 17% of the time, Pallas kernels for 0%

commit v1 on v0

v1 whole, which is shorter than its diff:
```python
import functools

import jax
import jax.numpy as jnp
from jax import lax
from jax.experimental import pallas as pl
from jax.experimental.pallas import tpu as pltpu
from jax.sharding import PartitionSpec as P

LANES = 128
F32 = jnp.float32
BF16 = jnp.bfloat16
ROWS_T = (((0,), (0,)), ((), ()))
COLS_T = (((1,), (1,)), ((), ()))


def barrier(n_ep, n_tp, me, tp):
    sem = pltpu.get_barrier_semaphore()
    for i in range(1, n_ep):
        pl.semaphore_signal(sem, inc=1, device_id={"ep": lax.rem(me + i, n_ep)})
    for i in range(1, n_tp):
        pl.semaphore_signal(sem, inc=1, device_id={"tp": lax.rem(tp + i, n_tp)})
    pl.semaphore_wait(sem, n_ep + n_tp - 2)


def remote(src, dst, send, recv, where):
    return pltpu.make_async_remote_copy(
        src_ref=src, dst_ref=dst, send_sem=send, recv_sem=recv, device_id=where
    )


def named_experts(routing, experts):
    ids = lax.broadcasted_iota(jnp.int32, (routing.shape[0], experts), 1)
    named = jnp.zeros(ids.shape, F32)
    for k in range(routing.shape[1]):
        named = jnp.maximum(named, (routing[:, k : k + 1] == ids).astype(F32))
    return named


def column(value, index):
    ids = lax.broadcasted_iota(jnp.int32, value.shape, 1)
    return jnp.sum(jnp.where(ids == index, value, 0.0), axis=1, keepdims=True)


def dispatch_kernel(
    dims, tok_ref, cot_ref, routing_ref, router_ref,
    rows_ref, cots_ref, scale_ref, aff_ref, pos_ref,
    stage, scale_stage, own_sem, sc_send, sc_recv, a_send, a_recv, y_send, y_recv, p_send, p_recv,
):
    n_ep, n_tp, n_batch, capacity, cap_pad, col_width = dims
    per = n_ep // n_batch
    n_y = n_tp // 2
    me = lax.axis_index("ep")
    tp = lax.axis_index("tp")
    y_at, core = tp // 2, lax.rem(tp, 2)
    partner = y_at * 2 + 1 - core
    experts = router_ref.shape[1]
    tok_count = tok_ref.shape[0]
    outs = (rows_ref, cots_ref)

    def cols(index):
        return pl.ds(pl.multiple_of(index * col_width, LANES), col_width)

    named = named_experts(routing_ref[...], experts)
    below = (
        lax.broadcasted_iota(jnp.int32, (tok_count, tok_count), 1)
        < lax.broadcasted_iota(jnp.int32, (tok_count, tok_count), 0)
    ).astype(BF16)
    pos = jnp.dot(below, named.astype(BF16), preferred_element_type=F32)
    logits = jnp.dot(tok_ref[...], router_ref[...], preferred_element_type=F32)
    aff = jax.nn.sigmoid(logits)
    total = jnp.sum(aff * named, axis=1, keepdims=True)
    weights = (aff * named / total).astype(BF16).astype(F32)
    aff_ref[...] = aff
    pos_ref[...] = pos
    token_cols = (tok_ref[:, cols(tp)], cot_ref[:, cols(tp)])
    slots = lax.broadcasted_iota(jnp.int32, (tok_count, cap_pad), 1).astype(F32)

    barrier(n_ep, n_tp, me, tp)
    for i in range(n_ep):
        dest = lax.rem(me + i, n_ep)
        pick = jnp.where(column(pos, dest) == slots, column(named, dest), 0.0)
        scale_stage[dest] = jnp.sum(pick * column(weights, dest), axis=0, keepdims=True)
        pick = pick.astype(BF16)
        for a in range(2):
            moved = lax.dot_general(pick, token_cols[a], ROWS_T, preferred_element_type=F32)
            stage[a, dest] = moved[:capacity].astype(BF16)
        for a in range(2):
            target = outs[a].at[me, :, cols(tp)]
            if i == 0:
                pltpu.make_async_copy(stage.at[a, dest], target, own_sem.at[a]).start()
            else:
                remote(
                    stage.at[a, dest], target, a_send.at[a, dest], a_recv.at[a, me], {"ep": dest}
                ).start()
        if i == 0:
            pltpu.make_async_copy(scale_stage.at[dest], scale_ref.at[me], own_sem.at[2]).start()
        else:
            remote(
                scale_stage.at[dest], scale_ref.at[me], sc_send.at[dest], sc_recv.at[me], {"ep": dest}
            ).start()

    def y_copy(a, batch, y_to):
        ref = outs[a].at[pl.ds(batch * per, per), :, cols(tp)]
        return remote(
            ref, ref, y_send.at[a, batch, y_to], y_recv.at[a, batch, y_at], {"tp": y_to * 2 + core}
        )

    def y_arrival(a, batch, y_from):
        ref = outs[a].at[pl.ds(batch * per, per), :, cols(y_from * 2 + core)]
        return remote(
            ref, ref, y_send.at[a, batch, y_from], y_recv.at[a, batch, y_from], {"tp": y_from * 2 + core}
        )

    def p_copy(a, batch, y_of):
        ref = outs[a].at[pl.ds(batch * per, per), :, cols(y_of * 2 + core)]
        return remote(ref, ref, p_send.at[a, batch, y_of], p_recv.at[a, batch, y_of], {"tp": partner})

    def p_arrival(a, batch, y_of):
        ref = outs[a].at[pl.ds(batch * per, per), :, cols(y_of * 2 + 1 - core)]
        return remote(ref, ref, p_send.at[a, batch, y_of], p_recv.at[a, batch, y_of], {"tp": partner})

    def relay(batch):
        for a in range(2):
            for j in range(1, n_y):
                y_from = lax.rem(y_at + j, n_y)
                y_arrival(a, batch, y_from).wait_recv()
                p_copy(a, batch, y_from).start()

    my_batch = me // per
    batches = [lax.rem(my_batch - i + n_batch, n_batch) for i in range(n_batch)]
    for i, batch in enumerate(batches):
        for a in range(2):
            for j in range(per):
                source = batch * per + j

                def from_other(a=a, source=source):
                    ref = outs[a].at[source, :, cols(tp)]
                    remote(
                        ref, ref, a_send.at[a, source], a_recv.at[a, source], {"ep": source}
                    ).wait_recv()

                def from_self(a=a, source=source):
                    pltpu.make_async_copy(
                        stage.at[a, source], outs[a].at[source, :, cols(tp)], own_sem.at[a]
                    ).wait()

                if per == 1:
                    (from_self if i == 0 else from_other)()
                elif i > 0:
                    from_other()
                else:
                    pl.when(source == me)(from_self)
                    pl.when(source != me)(from_other)
            for j in range(1, n_y):
                y_copy(a, batch, lax.rem(y_at + j, n_y)).start()
            p_copy(a, batch, y_at).start()
        if i > 1:
            relay(batches[i - 2])
    for batch in batches[-2:]:
        relay(batch)
    for batch in batches:
        for a in range(2):
            for j in range(n_y):
                p_arrival(a, batch, lax.rem(y_at + j, n_y)).wait_recv()
    for i in range(1, n_ep):
        other = lax.rem(me + i, n_ep)
        remote(
            scale_stage.at[other], scale_ref.at[other], sc_send.at[other], sc_recv.at[other], {"ep": other}
        ).wait()
        for a in range(2):
            remote(
                stage.at[a, other], outs[a].at[me, :, cols(tp)], a_send.at[a, other],
                a_recv.at[a, me], {"ep": other},
            ).wait_send()
    pltpu.make_async_copy(scale_stage.at[me], scale_ref.at[me], own_sem.at[2]).wait()
    for batch in batches:
        for a in range(2):
            for j in range(n_y):
                y_to = lax.rem(y_at + j, n_y)
                if j > 0:
                    y_copy(a, batch, y_to).wait_send()
                p_copy(a, batch, y_to).wait_send()


def combine_kernel(
    dims, part_ref, gate_ref, rowsq_ref, tok_ref, routing_ref, router_ref, aff_ref, pos_ref,
    token_ref, rgrad_ref, rrows_ref, rowsum_ref,
    r1, s1, r2, res, back, gate_in, gate_sum, gate_back, rowsq_in, rpart, rparts, tgrad,
    s1_send, s1_recv, s2_send, s2_recv, s3_send, s3_recv, gt_send, gt_recv, gb_send, gb_recv,
    rs_send, rs_recv, rp_send, rp_recv, ty_send, ty_recv, tp_send, tp_recv, own_sem,
):
    n_ep, n_tp, n_batch, capacity, cap_pad, col_width = dims
    per = n_ep // n_batch
    n_y = n_tp // 2
    me = lax.axis_index("ep")
    tp = lax.axis_index("tp")
    y_at, core = tp // 2, lax.rem(tp, 2)
    partner = y_at * 2 + 1 - core
    experts = router_ref.shape[1]
    tok_count = tok_ref.shape[0]

    def cols(index):
        return pl.ds(pl.multiple_of(index * col_width, LANES), col_width)

    def span(batch):
        return pl.ds(batch * per, per)

    my_batch = me // per
    batches = [lax.rem(my_batch + i + 1, n_batch) for i in range(n_batch)]
    barrier(n_ep, n_tp, me, tp)

    def first(batch, y_to):
        return remote(
            part_ref.at[span(batch), :, cols(y_to * 2 + 1 - core)], r1.at[y_to, span(batch)],
            s1_send.at[batch, y_to], s1_recv.at[batch, y_to], {"tp": partner},
        )

    def second(batch, y_to, y_from):
        return remote(
            s1.at[y_to, span(batch)], r2.at[y_from, span(batch)],
            s2_send.at[batch, y_to], s2_recv.at[batch, y_from], {"tp": y_to * 2 + core},
        )

    def third(dest, source):
        return remote(
            res.at[dest], back.at[source], s3_send.at[dest], s3_recv.at[source], {"ep": dest}
        )

    def gate_part(other, slot):
        return remote(gate_ref, gate_in.at[slot], gt_send.at[other], gt_recv.at[slot], {"tp": other})

    def gate_home(dest, source):
        return remote(
            gate_sum.at[dest], gate_back.at[source], gb_send.at[dest], gb_recv.at[source], {"ep": dest}
        )

    def squares(other, slot):
        return remote(rowsq_ref, rowsq_in.at[slot], rs_send.at[other], rs_recv.at[slot], {"tp": other})

    for i in range(1, n_tp):
        gate_part(lax.rem(tp + i, n_tp), tp).start()
    for batch in batches:
        for j in range(n_y):
            first(batch, lax.rem(y_at + n_y - 1 - j, n_y)).start()
    for i in range(1, n_tp):
        squares(lax.rem(tp + i, n_tp), tp).start()

    def reduce_core(batch):
        for j in range(n_y):
            y_to = lax.rem(y_at + n_y - 1 - j, n_y)
            first(batch, y_to).wait_recv()
            mine = part_ref[span(batch), :, cols(y_to * 2 + core)].astype(F32)
            s1[y_to, span(batch)] = (mine + r1[y_to, span(batch)].astype(F32)).astype(BF16)
            if j < n_y - 1:
                second(batch, y_to, y_at).start()

    def reduce_y(batch, is_own):
        total = s1[y_at, span(batch)].astype(F32)
        for j in range(1, n_y):
            y_from = lax.rem(y_at + j, n_y)
            second(batch, y_from, y_from).wait_recv()
            total = total + r2[y_from, span(batch)].astype(F32)
        res[span(batch)] = total.astype(BF16)
        for j in range(per):
            dest = batch * per + j

            def to_self(dest=dest):
                pltpu.make_async_copy(res.at[dest], back.at[dest], own_sem.at[0]).start()

            def to_other(dest=dest):
                third(dest, me).start()

            if per == 1:
                (to_self if is_own else to_other)()
            elif not is_own:
                to_other()
            else:
                pl.when(dest == me)(to_self)
                pl.when(dest != me)(to_other)

    for i, batch in enumerate(batches):
        reduce_core(batch)
        if i == 1:
            gate = gate_ref[...]
            for j in range(1, n_tp):
                other = lax.rem(tp + j, n_tp)
                gate_part(other, other).wait_recv()
                gate = gate + gate_in[other]
            gate_sum[...] = gate
            for j in range(1, n_ep):
                gate_home(lax.rem(me + j, n_ep), me).start()
        if i > 1:
            reduce_y(batches[i - 2], False)
    reduce_y(batches[-2], n_batch == 1)
    reduce_y(batches[-1], True)

    named = named_experts(routing_ref[...], experts)
    aff, pos = aff_ref[...], pos_ref[...]
    total = jnp.sum(aff * named, axis=1, keepdims=True)
    weights = aff * named / total
    slots = lax.broadcasted_iota(jnp.int32, (tok_count, cap_pad), 1).astype(F32)
    ids = lax.broadcasted_iota(jnp.int32, (tok_count, experts), 1)

    d_weights = jnp.zeros((tok_count, experts), F32)
    picks = []
    for i in range(n_ep):
        source = lax.rem(me + i, n_ep)
        if i == 0:
            terms = gate_sum[source]
        else:
            gate_home(source, source).wait_recv()
            terms = gate_back[source]
        terms = terms.astype(BF16).astype(F32)
        pick = jnp.where(column(pos, source) == slots, column(named, source), 0.0)
        term = jnp.sum(pick * terms, axis=1, keepdims=True)
        d_weights = jnp.where(ids == source, term, d_weights)
        picks.append(pick.astype(BF16))
    mean = jnp.sum(d_weights * weights, axis=1, keepdims=True)
    d_logits = ((d_weights - mean) / total * aff * (1.0 - aff) * named).astype(BF16)

    rpart[...] = lax.dot_general(d_logits, tok_ref[:, cols(tp)], ROWS_T, preferred_element_type=F32)

    def router_copy(dest, source):
        return remote(rpart, rparts.at[source], rp_send.at[dest], rp_recv.at[source], {"ep": dest})

    for i in range(1, n_ep):
        router_copy(lax.rem(me + i, n_ep), me).start()

    grad = lax.dot_general(
        d_logits, router_ref[pl.ds(pl.multiple_of(tp * col_width, LANES), col_width), :], COLS_T,
        preferred_element_type=F32,
    )
    for i in range(n_ep):
        source = lax.rem(me - i + n_ep, n_ep)
        if i == 0:
            pltpu.make_async_copy(res.at[me], back.at[me], own_sem.at[0]).wait()
        else:
            third(source, source).wait_recv()
        pick = picks[(n_ep - i) % n_ep][:, :capacity]
        grad = grad + jnp.dot(pick, back[source], preferred_element_type=F32)
    tgrad[...] = grad.astype(BF16)

    def to_y(y_to):
        return remote(
            tgrad, token_ref.at[:, cols(tp)], ty_send.at[y_to], ty_recv.at[y_at], {"tp": y_to * 2 + core}
        )

    def from_y(y_from):
        ref = token_ref.at[:, cols(y_from * 2 + core)]
        return remote(ref, ref, ty_send.at[y_from], ty_recv.at[y_from], {"tp": y_from * 2 + core})

    def own_pair():
        return remote(
            tgrad, token_ref.at[:, cols(tp)], tp_send.at[y_at], tp_recv.at[y_at], {"tp": partner}
        )

    def pair(y_of):
        ref = token_ref.at[:, cols(y_of * 2 + core)]
        return remote(ref, ref, tp_send.at[y_of], tp_recv.at[y_of], {"tp": partner})

    def pair_in(y_of):
        ref = token_ref.at[:, cols(y_of * 2 + 1 - core)]
        return remote(ref, ref, tp_send.at[y_of], tp_recv.at[y_of], {"tp": partner})

    for j in range(1, n_y):
        to_y(lax.rem(y_at + j, n_y)).start()
    own_pair().start()
    own = pltpu.make_async_copy(tgrad, token_ref.at[:, cols(tp)], own_sem.at[1])
    own.start()

    rgrad = rpart[...]
    for i in range(1, n_ep):
        source = lax.rem(me + i, n_ep)
        router_copy(source, source).wait_recv()
        rgrad = rgrad + rparts[source]
    rgrad_ref[...] = rgrad
    rrows_ref[...] = jnp.sum(rgrad * rgrad, axis=0, keepdims=True)
    sums = rowsq_ref[...]
    for i in range(1, n_tp):
        other = lax.rem(tp + i, n_tp)
        squares(other, other).wait_recv()
        sums = sums + rowsq_in[other]
    rowsum_ref[...] = sums

    for j in range(1, n_y):
        y_from = lax.rem(y_at + j, n_y)
        from_y(y_from).wait_recv()
        pair(y_from).start()
    for j in range(n_y):
        pair_in(lax.rem(y_at + j, n_y)).wait_recv()
    own.wait()
    own_pair().wait_send()
    for j in range(1, n_y):
        other = lax.rem(y_at + j, n_y)
        to_y(other).wait_send()
        pair(other).wait_send()
    for i in range(1, n_tp):
        other = lax.rem(tp + i, n_tp)
        gate_part(other, tp).wait_send()
        squares(other, tp).wait_send()
    for i in range(1, n_ep):
        other = lax.rem(me + i, n_ep)
        gate_home(other, me).wait_send()
        third(other, me).wait_send()
        router_copy(other, me).wait_send()
    for batch in batches:
        for j in range(n_y):
            y_to = lax.rem(y_at + j, n_y)
            first(batch, y_to).wait_send()
            if j > 0:
                second(batch, y_to, y_at).wait_send()


def expert_backward(rows_in, cots_in, slot_scale, w_gate, w_up, w_down):
    pre_gate = jnp.dot(rows_in, w_gate, preferred_element_type=F32)
    pre_up = jnp.dot(rows_in, w_up, preferred_element_type=F32)
    sigmoid_gate = jax.nn.sigmoid(pre_gate)
    hidden = (pre_gate * sigmoid_gate * pre_up).astype(BF16)
    back_proj = lax.dot_general(cots_in, w_down, COLS_T, preferred_element_type=F32)
    gate_term = jnp.sum(hidden.astype(F32) * back_proj, axis=1)
    scaled = slot_scale * back_proj
    grad_up_pre = (scaled * pre_gate * sigmoid_gate).astype(BF16)
    grad_gate_pre = (
        scaled * pre_up * sigmoid_gate * (1.0 + pre_gate * (1.0 - sigmoid_gate))
    ).astype(BF16)
    weighted = (slot_scale * cots_in.astype(F32)).astype(BF16)
    grad_down = lax.dot_general(hidden, weighted, ROWS_T, preferred_element_type=F32)
    grad_gate = lax.dot_general(rows_in, grad_gate_pre, ROWS_T, preferred_element_type=F32)
    grad_up = lax.dot_general(rows_in, grad_up_pre, ROWS_T, preferred_element_type=F32)
    partial_value = lax.dot_general(grad_gate_pre, w_gate, COLS_T, preferred_element_type=F32)
    partial_value = partial_value + lax.dot_general(
        grad_up_pre, w_up, COLS_T, preferred_element_type=F32
    )
    return partial_value.astype(BF16), gate_term, grad_gate, grad_up, grad_down


def per_device(tokens, routing, router_weight, gate_weight, up_weight, down_weight, cotangent):
    n_ep = lax.axis_size("ep")
    n_tp = lax.axis_size("tp")
    tok_count, width = tokens.shape
    top_count = routing.shape[1]
    experts = router_weight.shape[1]
    capacity = 7 * tok_count * top_count // (4 * experts)
    cap_pad = -(-capacity // LANES) * LANES
    slots = n_ep * capacity
    col_width = width // n_tp
    n_batch = min(n_ep, 8)
    n_y = n_tp // 2
    dims = (n_ep, n_tp, n_batch, capacity, cap_pad, col_width)
    vmem = pl.BlockSpec(memory_space=pltpu.VMEM)
    hbm = pl.BlockSpec(memory_space=pl.ANY)
    dma = pltpu.SemaphoreType.DMA

    rows, cots, scale, aff, pos = pl.pallas_call(
        functools.partial(dispatch_kernel, dims),
        out_shape=(
            jax.ShapeDtypeStruct((n_ep, capacity, width), BF16),
            jax.ShapeDtypeStruct((n_ep, capacity, width), BF16),
            jax.ShapeDtypeStruct((n_ep, 1, cap_pad), F32),
            jax.ShapeDtypeStruct((tok_count, experts), F32),
            jax.ShapeDtypeStruct((tok_count, experts), F32),
        ),
        in_specs=[vmem] * 4,
        out_specs=(hbm, hbm, vmem, vmem, vmem),
        scratch_shapes=[
            pltpu.VMEM((2, n_ep, capacity, col_width), BF16),
            pltpu.VMEM((n_ep, 1, cap_pad), F32),
            dma((3,)),
            dma((n_ep,)), dma((n_ep,)),
            dma((2, n_ep)), dma((2, n_ep)),
            dma((2, n_batch, n_y)), dma((2, n_batch, n_y)),
            dma((2, n_batch, n_y)), dma((2, n_batch, n_y)),
        ],
        compiler_params=pltpu.CompilerParams(collective_id=0, has_side_effects=True),
        name="dispatch",
    )(tokens, cotangent, routing, router_weight)

    slot_scale = scale[:, 0, :capacity].reshape(slots)[:, None]
    partial_value, gate_term, grad_gate, grad_up, grad_down = expert_backward(
        rows.reshape(slots, width), cots.reshape(slots, width), slot_scale,
        gate_weight[0], up_weight[0], down_weight[0],
    )
    gate_term = jnp.pad(
        gate_term.reshape(n_ep, 1, capacity), ((0, 0), (0, 0), (0, cap_pad - capacity))
    )
    row_squares = jnp.stack(
        [jnp.sum(grad_gate * grad_gate, axis=1), jnp.sum(grad_up * grad_up, axis=1)]
    ).reshape(2, width // LANES, LANES)
    down_rows = jnp.sum(grad_down * grad_down, axis=1)

    token_grad, router_grad, router_rows, row_sums = pl.pallas_call(
        functools.partial(combine_kernel, dims),
        out_shape=(
            jax.ShapeDtypeStruct((tok_count, width), BF16),
            jax.ShapeDtypeStruct((experts, col_width), F32),
            jax.ShapeDtypeStruct((1, col_width), F32),
            jax.ShapeDtypeStruct(row_squares.shape, F32),
        ),
        in_specs=[vmem] * 8,
        out_specs=(hbm, vmem, vmem, vmem),
        scratch_shapes=[
            pltpu.VMEM((n_y, n_ep, capacity, col_width), BF16),
            pltpu.VMEM((n_y, n_ep, capacity, col_width), BF16),
            pltpu.VMEM((n_y, n_ep, capacity, col_width), BF16),
            pltpu.VMEM((n_ep, capacity, col_width), BF16),
            pltpu.VMEM((n_ep, capacity, col_width), BF16),
            pltpu.VMEM((n_tp, n_ep, 1, cap_pad), F32),
            pltpu.VMEM((n_ep, 1, cap_pad), F32),
            pltpu.VMEM((n_ep, 1, cap_pad), F32),
            pltpu.VMEM((n_tp,) + row_squares.shape, F32),
            pltpu.VMEM((experts, col_width), F32),
            pltpu.VMEM((n_ep, experts, col_width), F32),
            pltpu.VMEM((tok_count, col_width), BF16),
            dma((n_batch, n_y)), dma((n_batch, n_y)),
            dma((n_batch, n_y)), dma((n_batch, n_y)),
            dma((n_ep,)), dma((n_ep,)),
            dma((n_tp,)), dma((n_tp,)),
            dma((n_ep,)), dma((n_ep,)),
            dma((n_tp,)), dma((n_tp,)),
            dma((n_ep,)), dma((n_ep,)),
            dma((n_y,)), dma((n_y,)),
            dma((n_y,)), dma((n_y,)),
            dma((2,)),
        ],
        compiler_params=pltpu.CompilerParams(collective_id=1, has_side_effects=True),
        name="combine",
    )(partial_value.reshape(n_ep, capacity, width), gate_term, row_squares, tokens, routing,
      router_weight, aff, pos)

    row_sums = row_sums.reshape(2, 1, width)
    return (
        token_grad,
        router_grad.T,
        router_rows[0],
        grad_gate.astype(BF16)[None],
        grad_up.astype(BF16)[None],
        grad_down.astype(BF16)[None],
        row_sums[0],
        row_sums[1],
        down_rows[None],
    )


def solution(mesh):
    return jax.shard_map(
        per_device,
        mesh=mesh,
        in_specs=(
            P("ep", None),
            P("ep", None),
            P(),
            P("ep", None, "tp"),
            P("ep", None, "tp"),
            P("ep", "tp", None),
            P("ep", None),
        ),
        out_specs=(
            P("ep", None),
            P("tp", None),
            P("tp"),
            P("ep", None, "tp"),
            P("ep", None, "tp"),
            P("ep", "tp", None),
            P("ep", None),
            P("ep", None),
            P("ep", "tp"),
        ),
        check_vma=False,
    )
```

time: 256 us -> 116 us (0.45)
  waiting for transfers between devices: 90.1 us -> 0 us
  Pallas kernels: 0 us -> 72.1 us
  blocking collectives: 55 us -> 0 us
  starting transfers between devices: 26.2 us -> 0 us
  local copies, waits for them, and re-layouts: 30 us -> 15 us
  between operations: 14.3 us -> 0.71 us
  matrix products: 33.1 us -> 26 us
  other arithmetic: 6.23 us -> 0.61 us
    all_to_all x5 -> x0, waiting for transfers between devices: 74.4 us -> none  [the longest x1 37.2 us: per_device(): lax.all_to_all(rows_send, 'ep', split_axis=1, concat_axis=1, tiled=True)]
    pallas_call x0 -> x2, Pallas kernels: none -> 72.1 us  [the longest x1 40.1 us: per_device(): pl.pallas_call(functools.partial(dispatch_kernel, dims), out_shape=(jax.S...]
    psum x2 -> x0, blocking collectives: 48.5 us -> none  [the longest x1 37.5 us: per_device(): router_grad = lax.psum(router_part, 'ep')]
    all_to_all x5 -> x0, starting transfers between devices: 26 us -> none  [the longest x1 7.28 us: per_device(): lax.all_to_all(scale_send, 'ep', split_axis=1, concat_axis=1, tiled=True)]
    reduce_scatter x1 -> x0, waiting for transfers between devices: 15.6 us -> none  [per_device(): lax.psum_scatter(partial_value, 'tp', scatter_dimension=2, tiled=True)]
    gather x10 -> x0, local copies, waits for them, and re-layouts: 14.5 us -> none  [the longest x1 3.2 us: per_device(): tok_pad[source_tok].reshape(local_experts, groups, capacity, model_width)]
    dot_general x11 -> x8, matrix products: 33.1 us -> 26 us  [the longest x1 4.86 us: expert_backward(): lax.dot_general(hidden, weighted, ROWS_T, preferred_element_type=F32)]
    all_gather x1 -> x0, blocking collectives: 6.5 us -> none  [per_device(): token_grad = lax.all_gather(token_grad, 'tp', axis=1, tiled=True)]
  transfers between devices with their start and end apart: 6 -> 0, of which waited for: 4 -> 0; matrix products, arithmetic and copies ran while one was open for 17% -> 0% of each run, Pallas kernels for 0% -> 0%
where the time goes in v1:
time: 116 us; the launch traced here: 114 us
  Pallas kernels  72.1 us (62%)
  matrix products  26 us (22%)
  local copies, waits for them, and re-layouts  15 us (13%)
    pallas_call x1, Pallas kernels, per_device(): pl.pallas_call(functools.partial(dispatch_kernel, dims), out_shape=(jax.S...  40.1 us
    pallas_call x1, Pallas kernels, per_device(): pl.pallas_call(functools.partial(combine_kernel, dims), out_shape=(jax.Sh...  31.9 us
    unnamed x25, local copies, waits for them, and re-layouts  13.6 us
    dot_general x1, matrix products, expert_backward(): lax.dot_general(hidden, weighted, ROWS_T, preferred_element_type=F32)  4.86 us
    dot_general x1, matrix products, expert_backward(): pre_up = jnp.dot(rows_in, w_up, preferred_element_type=F32)  4.31 us
    dot_general x1, matrix products, expert_backward(): lax.dot_general(rows_in, grad_up_pre, ROWS_T, preferred_element_type=F32)  4.27 us
    dot_general x1, matrix products, expert_backward(): lax.dot_general(cots_in, w_down, COLS_T, preferred_element_type=F32)  4.27 us
    dot_general x1, matrix products, expert_backward(): lax.dot_general(rows_in, grad_gate_pre, ROWS_T, preferred_element_type=F32)  2.65 us

profile of v1, /device:TPU:0, one launch (start us, length us, event | category | flops | bytes accessed | tf_op | source)
XLA Modules:
  0.0 114.4 jit_solution(11938862222145416315)
XLA Ops:
  0.6 0.0 copy-start
  0.7 1.6 %copy.16.routing_ref = s32[128,2]{1,0:T(8,128)} copy(s32[128,2]{0,1:T(2,128)} %param.8) | data formatting | bytes 2048 | tf_op args[1]
  2.2 1.8 %copy.17.router_ref = bf16[2048,8]{1,0:T(8,128)(2,1)} copy(bf16[2048,8]{0,1:T(8,128)(2,1)} %param.9) | data formatting | bytes 65536 | tf_op args[2]
  4.0 40.1 %dispatch.1 = (bf16[8,56,2048]{2,1,0:T(8,128)(2,1)}, bf16[8,56,2048]{2,1,0:T(8,128)(2,1)}, f32[8,1,128]{2,1,0:T(1,128)}, f32[128,8]{1,0:T(8,128)}, f32[128,8]{1,0:T(8,128)}) custom-call(bf16[128,2048]{1,0:T(8,128)(2,1)} %tok_ref.3, bf16[128,2048]{1,0:T(8,128)(2,1)} %cot_ref.1, s32[128,2]{1,0:T(8,128)} %copy.16.routing_ref, bf16[2048,8]{1,0:T(8,128)(2,1)} %copy.17.router_ref), custom_call_target="tpu_custom_call" | custom-call | tf_op jit(solution)/shard_map/dispatch/pallas_call | solution.py:455
  44.1 0.0 copy-start.7
  44.1 4.3 %fusion.5 = f32[448,512]{1,0:T(8,128)} fusion(bf16[448,2048]{1,0:T(8,128)(2,1)} %bitcast.50, bf16[1,2048,512]{2,1,0:T(8,128)(2,1)} %param.11), kind=kOutput, calls=%fused_computation.10 | convolution fusion | flops 939524096 | bytes 4849664 | tf_op jit(solution)/shard_map/dot_general | solution.py:417
  48.4 0.0 copy-done
  48.4 0.0 copy-done.7
  48.4 0.0 copy-start.5
  48.4 2.1 %fusion.2 = f32[448,512]{1,0:T(8,128)} fusion(bf16[448,2048]{1,0:T(8,128)(2,1)S(1)} %bitcast.52, bf16[1,2048,512]{2,1,0:T(8,128)(2,1)S(1)} %copy-done), kind=kOutput, calls=%fused_computation.7 | convolution fusion | flops 939524096 | bytes 4849664 | tf_op jit(solution)/shard_map/dot_general | solution.py:416
  50.5 0.0 copy-done.5
  50.5 0.1 mul.54
  50.6 4.3 %multiply_reduce_fusion.3 = (f32[448]{0:T(512)S(1)}, bf16[448,512]{1,0:T(8,128)(2,1)S(1)}, bf16[448,512]{1,0:T(8,128)(2,1)S(1)}, bf16[448,512]{1,0:T(8,128)(2,1)S(1)}) fusion(f32[448,512]{1,0:T(8,128)} %fusion.5, f32[448,512]{1,0:T(8,128)} %fusion.2, f32[448]{0:T(512)S(1)} %mul.54, bf16[448,2048]{1,0:T(8,128)(2,1)} %bitcast.48, bf16[1,512,2048]{2,1,0:T(8,128)(2,1)} %param.12), kind=kOutput, calls=%fused_computation.19 | convolution fusion | flops 944111168 | bytes 7147008 | tf_op jit(solution)/shard_map/dot_general | solution.py:420
  54.9 0.0 copy-start.1
  54.9 1.2 %fusion = f32[448,2048]{1,0:T(8,128)S(1)} fusion(bf16[448,512]{1,0:T(8,128)(2,1)S(1)} %get-tuple-element.44, bf16[1,2048,512]{2,1,0:T(8,128)(2,1)S(1)} %copy-done), kind=kOutput, calls=%fused_computation.5 | convolution fusion | flops 939524096 | bytes 6225920 | tf_op jit(solution)/shard_map/dot_general | solution.py:431
  56.1 0.4 copy-done.1
  56.5 2.4 %add_convert_fusion = bf16[448,2048]{1,0:T(8,128)(2,1)} fusion(f32[448,2048]{1,0:T(8,128)S(1)} %fusion, bf16[448,512]{1,0:T(8,128)(2,1)S(1)} %get-tuple-element.45, bf16[1,2048,512]{2,1,0:T(8,128)(2,1)S(1)} %copy-done.1), kind=kOutput, calls=%fused_computation.4 | convolution fusion | flops 941359104 | bytes 8060928 | tf_op jit(solution)/shard_map/dot_general | solution.py:432
  58.9 0.1 reshape.44
  59.0 0.6 pad.4.gate_ref
  59.6 0.0 copy-start.8
  59.6 4.3 %convert_bitcast_fusion.1 = (bf16[1,2048,512]{1,2,0:T(8,128)(2,1)}, f32[2048]{0:T(1024)S(1)}) fusion(bf16[448,2048]{1,0:T(8,128)(2,1)} %bitcast.51, bf16[448,512]{1,0:T(8,128)(2,1)S(1)} %get-tuple-element.45), kind=kOutput, calls=%fused_computation.15 | convolution fusion | flops 942667776 | bytes 4399104 | tf_op jit(solution)/shard_map/dot_general | solution.py:430
  63.8 0.0 copy-done.8
  63.8 2.7 %convert_bitcast_fusion.2 = (bf16[1,2048,512]{1,2,0:T(8,128)(2,1)}, f32[2048]{0:T(1024)S(1)}) fusion(bf16[448,2048]{1,0:T(8,128)(2,1)S(1)} %bitcast.53, bf16[448,512]{1,0:T(8,128)(2,1)S(1)} %get-tuple-element.44), kind=kOutput, calls=%fused_computation.16 | convolution fusion | flops 942667776 | bytes 4399104 | tf_op jit(solution)/shard_map/dot_general | solution.py:429
  66.5 0.6 pad_maximum_fusion.rowsq_ref
  67.1 31.9 %combine.1 = (bf16[128,2048]{1,0:T(8,128)(2,1)}, f32[8,512]{1,0:T(8,128)}, f32[1,512]{1,0:T(1,128)}, f32[2,16,128]{2,1,0:T(8,128)}) custom-call(bf16[8,56,2048]{2,1,0:T(8,128)(2,1)} %bitcast.41, f32[8,1,128]{2,1,0:T(1,128)} %pad.4.gate_ref, f32[2,16,128]{2,1,0:T(8,128)} %pad_maximum_fusion.rowsq_ref, bf16[128,2048]{1,0:T(8,128)(2,1)} %tok_ref.3, ...), custom_call_target="tpu_custom_call" | custom-call | tf_op jit(solution)/shard_map/combine/pallas_call | solution.py:492
  99.1 3.9 %copy.20 = bf16[1,2048,512]{2,1,0:T(8,128)(2,1)} copy(bf16[1,2048,512]{1,2,0:T(8,128)(2,1)} %get-tuple-element.42) | data formatting | bytes 4194304
  103.0 3.9 %copy.21 = bf16[1,2048,512]{2,1,0:T(8,128)(2,1)} copy(bf16[1,2048,512]{1,2,0:T(8,128)(2,1)} %get-tuple-element.40) | data formatting | bytes 4194304
  106.9 0.0 copy-start.4
  106.9 0.0 copy-start.2
  106.9 0.0 copy-start.3
  106.9 0.0 copy-start.6
  106.9 4.9 %multiply_reduce_fusion = (f32[512]{0:T(512)}, bf16[1,512,2048]{2,1,0:T(8,128)(2,1)}) fusion(bf16[448,512]{1,0:T(8,128)(2,1)S(1)} %get-tuple-element.37, bf16[448,2048]{1,0:T(8,128)(2,1)} %bitcast.49, f32[448]{0:T(512)S(1)} %mul.54), kind=kOutput, calls=%fused_computation | convolution fusion | flops 945421824 | bytes 4394752 | tf_op jit(solution)/shard_map/dot_general | solution.py:428
  111.8 0.0 copy-done.4
  111.8 0.6 fusion.11
  112.4 0.0 copy-done.2
  112.4 0.8 copy.25
  113.2 0.0 copy-done.3
  113.2 0.6 copy.26
  113.8 0.0 copy-done.6
  113.8 0.6 copy.27
  (1 shorter events, 0.0 us)
Async XLA Ops:
  0.6 47.8 %copy-start = (bf16[1,2048,512]{2,1,0:T(8,128)(2,1)S(1)}, bf16[1,2048,512]{2,1,0:T(8,128)(2,1)}, u32[]{:S(2)}) copy-start(bf16[1,2048,512]{2,1,0:T(8,128)(2,1)} %param.10) | copy-start | bytes 6291460
  44.1 4.3 %copy-start.7 = (bf16[8,56,2048]{2,1,0:T(8,128)(2,1)S(1)}, bf16[8,56,2048]{2,1,0:T(8,128)(2,1)}, u32[]{:S(2)}) copy-start(bf16[8,56,2048]{2,1,0:T(8,128)(2,1)} %get-tuple-element.20) | copy-start | bytes 5505028
  48.4 2.1 %copy-start.5 = (f32[8,1,128]{2,1,0:T(1,128)S(1)}, f32[8,1,128]{2,1,0:T(1,128)}, u32[]{:S(2)}) copy-start(f32[8,1,128]{2,1,0:T(1,128)} %get-tuple-element.18) | copy-start | bytes 12292
  54.9 1.6 %copy-start.1 = (bf16[1,2048,512]{2,1,0:T(8,128)(2,1)S(1)}, bf16[1,2048,512]{2,1,0:T(8,128)(2,1)}, u32[]{:S(2)}) copy-start(bf16[1,2048,512]{2,1,0:T(8,128)(2,1)} %param.11) | copy-start | bytes 6291460
  59.6 4.3 %copy-start.8 = (bf16[8,56,2048]{2,1,0:T(8,128)(2,1)S(1)}, bf16[8,56,2048]{2,1,0:T(8,128)(2,1)}, u32[]{:S(2)}) copy-start(bf16[8,56,2048]{2,1,0:T(8,128)(2,1)} %get-tuple-element.20) | copy-start | bytes 5505028
  106.9 4.9 %copy-start.4 = (f32[2,16,128]{2,1,0:T(8,128)S(1)}, f32[2,16,128]{2,1,0:T(8,128)}, u32[]{:S(2)}) copy-start(f32[2,16,128]{2,1,0:T(8,128)} %get-tuple-element.26) | copy-start | bytes 49156
  106.9 5.5 %copy-start.2 = (bf16[128,2048]{1,0:T(8,128)(2,1)S(1)}, bf16[128,2048]{1,0:T(8,128)(2,1)}, u32[]{:S(2)}) copy-start(bf16[128,2048]{1,0:T(8,128)(2,1)} %get-tuple-element.57) | copy-start | bytes 1572868
  106.9 6.3 %copy-start.3 = (f32[8,512]{1,0:T(8,128)S(1)}, f32[8,512]{1,0:T(8,128)}, u32[]{:S(2)}) copy-start(f32[8,512]{1,0:T(8,128)} %get-tuple-element.24) | copy-start | bytes 49156
  106.9 6.9 %copy-start.6 = (f32[1,512]{1,0:T(1,128)S(1)}, f32[1,512]{1,0:T(1,128)}, u32[]{:S(2)}) copy-start(f32[1,512]{1,0:T(1,128)} %get-tuple-element.25) | copy-start | bytes 6148

commit v2 on v1

--- a/solution.py
+++ b/solution.py
@@ -30,11 +30,11 @@
 
 
 def named_experts(routing, experts):
-    ids = lax.broadcasted_iota(jnp.int32, (routing.shape[0], experts), 1)
+    ids = lax.broadcasted_iota(jnp.int32, (experts, routing.shape[1]), 0)
     named = jnp.zeros(ids.shape, F32)
-    for k in range(routing.shape[1]):
-        named = jnp.maximum(named, (routing[:, k : k + 1] == ids).astype(F32))
-    return named
+    for k in range(routing.shape[0]):
+        named = jnp.maximum(named, (routing[k : k + 1, :] == ids).astype(F32))
+    return named.T
 
 
 def column(value, index):
@@ -54,7 +54,7 @@
     tp = lax.axis_index("tp")
     y_at, core = tp // 2, lax.rem(tp, 2)
     partner = y_at * 2 + 1 - core
-    experts = router_ref.shape[1]
+    experts = router_ref.shape[0]
     tok_count = tok_ref.shape[0]
     outs = (rows_ref, cots_ref)
 
@@ -67,7 +67,7 @@
         < lax.broadcasted_iota(jnp.int32, (tok_count, tok_count), 0)
     ).astype(BF16)
     pos = jnp.dot(below, named.astype(BF16), preferred_element_type=F32)
-    logits = jnp.dot(tok_ref[...], router_ref[...], preferred_element_type=F32)
+    logits = lax.dot_general(tok_ref[...], router_ref[...], COLS_T, preferred_element_type=F32)
     aff = jax.nn.sigmoid(logits)
     total = jnp.sum(aff * named, axis=1, keepdims=True)
     weights = (aff * named / total).astype(BF16).astype(F32)
@@ -197,7 +197,7 @@
     tp = lax.axis_index("tp")
     y_at, core = tp // 2, lax.rem(tp, 2)
     partner = y_at * 2 + 1 - core
-    experts = router_ref.shape[1]
+    experts = router_ref.shape[0]
     tok_count = tok_ref.shape[0]
 
     def cols(index):
@@ -327,10 +327,7 @@
     for i in range(1, n_ep):
         router_copy(lax.rem(me + i, n_ep), me).start()
 
-    grad = lax.dot_general(
-        d_logits, router_ref[pl.ds(pl.multiple_of(tp * col_width, LANES), col_width), :], COLS_T,
-        preferred_element_type=F32,
-    )
+    grad = jnp.dot(d_logits, router_ref[:, cols(tp)], preferred_element_type=F32)
     for i in range(n_ep):
         source = lax.rem(me - i + n_ep, n_ep)
         if i == 0:
@@ -412,6 +409,40 @@
                 second(batch, y_to, y_at).wait_send()
 
 
+def lane_squares(value):
+    squares = value * value
+    total = squares[:, :LANES]
+    for at in range(LANES, value.shape[1], LANES):
+        total = total + squares[:, at : at + LANES]
+    return total
+
+
+def weight_grad_kernel(
+    rows_ref, cots_ref, hidden_ref, gate_ref, up_ref, scale_ref,
+    gate_out, up_out, down_out, squares_out, down_squares_out, hidden_t, down_acc,
+):
+    step = pl.program_id(0)
+
+    @pl.when(step == 0)
+    def _():
+        hidden_t[...] = hidden_ref[...].T
+        down_acc[...] = jnp.zeros_like(down_acc)
+
+    rows_t = rows_ref[...].T
+    for a, (pre, out) in enumerate(((gate_ref, gate_out), (up_ref, up_out))):
+        grad = jnp.dot(rows_t, pre[...], preferred_element_type=F32)
+        out[...] = grad.astype(BF16)
+        squares_out[a] = jnp.sum(lane_squares(grad).T, axis=0, keepdims=True)
+    weighted = (scale_ref[...] * cots_ref[...].astype(F32)).astype(BF16)
+    grad = jnp.dot(hidden_t[...], weighted, preferred_element_type=F32)
+    down_out[...] = grad.astype(BF16)
+    down_acc[...] += lane_squares(grad)
+
+    @pl.when(step == pl.num_programs(0) - 1)
+    def _():
+        down_squares_out[...] = jnp.sum(down_acc[...].T, axis=0, keepdims=True)
+
+
 def expert_backward(rows_in, cots_in, slot_scale, w_gate, w_up, w_down):
     pre_gate = jnp.dot(rows_in, w_gate, preferred_element_type=F32)
     pre_up = jnp.dot(rows_in, w_up, preferred_element_type=F32)
@@ -424,15 +455,11 @@
     grad_gate_pre = (
         scaled * pre_up * sigmoid_gate * (1.0 + pre_gate * (1.0 - sigmoid_gate))
     ).astype(BF16)
-    weighted = (slot_scale * cots_in.astype(F32)).astype(BF16)
-    grad_down = lax.dot_general(hidden, weighted, ROWS_T, preferred_element_type=F32)
-    grad_gate = lax.dot_general(rows_in, grad_gate_pre, ROWS_T, preferred_element_type=F32)
-    grad_up = lax.dot_general(rows_in, grad_up_pre, ROWS_T, preferred_element_type=F32)
     partial_value = lax.dot_general(grad_gate_pre, w_gate, COLS_T, preferred_element_type=F32)
     partial_value = partial_value + lax.dot_general(
         grad_up_pre, w_up, COLS_T, preferred_element_type=F32
     )
-    return partial_value.astype(BF16), gate_term, grad_gate, grad_up, grad_down
+    return partial_value.astype(BF16), gate_term, hidden, grad_gate_pre, grad_up_pre
 
 
 def per_device(tokens, routing, router_weight, gate_weight, up_weight, down_weight, cotangent):
@@ -474,20 +501,47 @@
         ],
         compiler_params=pltpu.CompilerParams(collective_id=0, has_side_effects=True),
         name="dispatch",
-    )(tokens, cotangent, routing, router_weight)
+    )(tokens, cotangent, routing.T, router_weight.T)
 
     slot_scale = scale[:, 0, :capacity].reshape(slots)[:, None]
-    partial_value, gate_term, grad_gate, grad_up, grad_down = expert_backward(
-        rows.reshape(slots, width), cots.reshape(slots, width), slot_scale,
+    rows, cots = rows.reshape(slots, width), cots.reshape(slots, width)
+    partial_value, gate_term, hidden, grad_gate_pre, grad_up_pre = expert_backward(
+        rows, cots, slot_scale,
         gate_weight[0], up_weight[0], down_weight[0],
     )
     gate_term = jnp.pad(
         gate_term.reshape(n_ep, 1, capacity), ((0, 0), (0, 0), (0, cap_pad - capacity))
     )
-    row_squares = jnp.stack(
-        [jnp.sum(grad_gate * grad_gate, axis=1), jnp.sum(grad_up * grad_up, axis=1)]
-    ).reshape(2, width // LANES, LANES)
-    down_rows = jnp.sum(grad_down * grad_down, axis=1)
+    span = 2 * LANES if width % (2 * LANES) == 0 else LANES
+    units = hidden.shape[1]
+    whole = pl.BlockSpec((slots, units), lambda i: (0, 0))
+    grad_gate, grad_up, grad_down, row_squares, down_rows = pl.pallas_call(
+        weight_grad_kernel,
+        grid=(width // span,),
+        out_shape=(
+            jax.ShapeDtypeStruct((width, units), BF16),
+            jax.ShapeDtypeStruct((width, units), BF16),
+            jax.ShapeDtypeStruct((units, width), BF16),
+            jax.ShapeDtypeStruct((2, 1, width), F32),
+            jax.ShapeDtypeStruct((1, units), F32),
+        ),
+        in_specs=[
+            pl.BlockSpec((slots, span), lambda i: (0, i)),
+            pl.BlockSpec((slots, span), lambda i: (0, i)),
+            whole, whole, whole,
+            pl.BlockSpec((slots, 1), lambda i: (0, 0)),
+        ],
+        out_specs=(
+            pl.BlockSpec((span, units), lambda i: (i, 0)),
+            pl.BlockSpec((span, units), lambda i: (i, 0)),
+            pl.BlockSpec((units, span), lambda i: (0, i)),
+            pl.BlockSpec((2, 1, span), lambda i: (0, 0, i)),
+            pl.BlockSpec((1, units), lambda i: (0, 0)),
+        ),
+        scratch_shapes=[pltpu.VMEM((units, slots), BF16), pltpu.VMEM((units, LANES), F32)],
+        compiler_params=pltpu.CompilerParams(dimension_semantics=("arbitrary",)),
+        name="weight_grads",
+    )(rows, cots, hidden, grad_gate_pre, grad_up_pre, slot_scale)
 
     token_grad, router_grad, router_rows, row_sums = pl.pallas_call(
         functools.partial(combine_kernel, dims),
@@ -525,20 +579,19 @@
         ],
         compiler_params=pltpu.CompilerParams(collective_id=1, has_side_effects=True),
         name="combine",
-    )(partial_value.reshape(n_ep, capacity, width), gate_term, row_squares, tokens, routing,
-      router_weight, aff, pos)
-
-    row_sums = row_sums.reshape(2, 1, width)
+    )(partial_value.reshape(n_ep, capacity, width), gate_term, row_squares, tokens,
+      routing.T, router_weight.T, aff, pos)
+
     return (
         token_grad,
         router_grad.T,
         router_rows[0],
-        grad_gate.astype(BF16)[None],
-        grad_up.astype(BF16)[None],
-        grad_down.astype(BF16)[None],
+        grad_gate[None],
+        grad_up[None],
+        grad_down[None],
         row_sums[0],
         row_sums[1],
-        down_rows[None],
+        down_rows,
     )
 
 

time: 116 us -> 106 us (0.914)
  matrix products: 26 us -> 13.4 us
  Pallas kernels: 72.1 us -> 82.2 us
  local copies, waits for them, and re-layouts: 15 us -> 7.84 us
    dot_general x3 -> x0, matrix products: 11.8 us -> none  [the longest x1 4.86 us: expert_backward(): lax.dot_general(hidden, weighted, ROWS_T, preferred_element_type=F32)]
    pallas_call x0 -> x1, Pallas kernels: none -> 10.3 us  [per_device(): pl.pallas_call(weight_grad_kernel, grid=(width // span,), out_shape=(jax....]
    unnamed x25 -> x17, local copies, waits for them, and re-layouts: 13.6 us -> 4.92 us
    dot_general x1, matrix products: 4.31 us -> 2.04 us  [expert_backward(): pre_up = jnp.dot(rows_in, w_up, preferred_element_type=F32)]
    squeeze x0 -> x1, local copies, waits for them, and re-layouts: none -> 1.32 us  [per_device(): row_sums[1]]
where the time goes in v2:
time: 106 us; the launch traced here: 104 us
  Pallas kernels  82.2 us (78%)
  matrix products  13.4 us (13%)
  local copies, waits for them, and re-layouts  7.84 us (7%)
    pallas_call x1, Pallas kernels, per_device(): pl.pallas_call(functools.partial(dispatch_kernel, dims), out_shape=(jax.S...  40.1 us
    pallas_call x1, Pallas kernels, per_device(): pl.pallas_call(functools.partial(combine_kernel, dims), out_shape=(jax.Sh...  31.8 us
    pallas_call x1, Pallas kernels, per_device(): pl.pallas_call(weight_grad_kernel, grid=(width // span,), out_shape=(jax....  10.3 us
    dot_general x1, matrix products, expert_backward(): lax.dot_general(cots_in, w_down, COLS_T, preferred_element_type=F32)  5 us
    unnamed x17, local copies, waits for them, and re-layouts  4.92 us
    dot_general x1, matrix products, expert_backward(): pre_gate = jnp.dot(rows_in, w_gate, preferred_element_type=F32)  2.75 us
    dot_general x1, matrix products, expert_backward(): lax.dot_general(grad_up_pre, w_up, COLS_T, preferred_element_type=F32)  2.39 us

profile of v2, /device:TPU:0, one launch (start us, length us, event | category | flops | bytes accessed | tf_op | source)
XLA Modules:
  0.0 104.2 jit_solution(14404821727795305603)
XLA Ops:
  0.6 0.0 copy-start
  0.7 40.1 %dispatch.1 = (bf16[8,56,2048]{2,1,0:T(8,128)(2,1)}, bf16[8,56,2048]{2,1,0:T(8,128)(2,1)}, f32[8,1,128]{2,1,0:T(1,128)}, f32[128,8]{1,0:T(8,128)}, f32[128,8]{1,0:T(8,128)}) custom-call(bf16[128,2048]{1,0:T(8,128)(2,1)} %tok_ref.3, bf16[128,2048]{1,0:T(8,128)(2,1)} %cot_ref.1, s32[2,128]{1,0:T(2,128)} %bitcast.45, bf16[8,2048]{1,0:T(8,128)(2,1)} %bitcast.41), custom_call_target="tpu_custom_call" | custom-call | tf_op jit(solution)/shard_map/dispatch/pallas_call | solution.py:482
  40.8 0.0 copy-done
  40.8 0.0 copy-start.2
  40.8 0.0 copy-start.4
  40.8 2.8 %fusion.2 = f32[448,512]{1,0:T(8,128)S(1)} fusion(bf16[448,2048]{1,0:T(8,128)(2,1)} %bitcast.36, bf16[1,2048,512]{2,1,0:T(8,128)(2,1)S(1)} %copy-done), kind=kOutput, calls=%fused_computation.3 | convolution fusion | flops 939524096 | bytes 4849664 | tf_op jit(solution)/shard_map/dot_general | solution.py:447
  43.6 0.0 copy-done.2
  43.6 0.0 copy-done.4
  43.6 0.0 copy-start.6
  43.6 2.0 %fusion.5 = f32[448,512]{1,0:T(8,128)} fusion(bf16[448,2048]{1,0:T(8,128)(2,1)S(1)} %bitcast.38, bf16[1,2048,512]{2,1,0:T(8,128)(2,1)S(1)} %copy-done.2), kind=kOutput, calls=%fused_computation.6 | convolution fusion | flops 939524096 | bytes 4849664 | tf_op jit(solution)/shard_map/dot_general | solution.py:448
  45.6 0.0 copy-done.6
  45.6 0.1 mul.37
  45.7 5.0 %multiply_reduce_fusion = (f32[448]{0:T(512)S(1)}, bf16[448,512]{1,0:T(8,128)(2,1)}, bf16[448,512]{1,0:T(8,128)(2,1)}, bf16[448,512]{1,0:T(8,128)(2,1)}) fusion(f32[448,512]{1,0:T(8,128)} %fusion.5, f32[448,512]{1,0:T(8,128)S(1)} %fusion.2, f32[448]{0:T(512)S(1)} %mul.37, bf16[448,2048]{1,0:T(8,128)(2,1)} %bitcast.39, bf16[1,512,2048]{2,1,0:T(8,128)(2,1)} %param.12), kind=kOutput, calls=%fused_computation.10 | convolution fusion | flops 944111168 | bytes 7147008 | tf_op jit(solution)/shard_map/dot_general | solution.py:451
  50.7 0.8 broadcast_in_dim_reshape_squeeze.4.scale_ref
  51.5 0.0 copy-start.1
  51.5 10.3 %weight_grads.1 = (bf16[2048,512]{1,0:T(8,128)(2,1)}, bf16[2048,512]{1,0:T(8,128)(2,1)}, bf16[512,2048]{1,0:T(8,128)(2,1)}, f32[2,1,2048]{2,1,0:T(1,128)}, f32[1,512]{1,0:T(1,128)}) custom-call(bf16[448,2048]{1,0:T(8,128)(2,1)} %bitcast.37, bf16[448,2048]{1,0:T(8,128)(2,1)} %bitcast.40, bf16[448,512]{1,0:T(8,128)(2,1)} %get-tuple-element.38.hidden_ref, ...), custom_call_target="tpu_custom_call" | custom-call | tf_op jit(solution)/shard_map/weight_grads/pallas_call | solution.py:518
  61.8 0.0 copy-done.1
  61.8 0.0 copy-start.3
  61.8 0.0 copy-start.5
  61.9 1.2 %fusion = f32[448,2048]{1,0:T(8,128)S(1)} fusion(bf16[448,512]{1,0:T(8,128)(2,1)S(1)} %copy-done.1, bf16[1,2048,512]{2,1,0:T(8,128)(2,1)S(1)} %copy-done), kind=kOutput, calls=%fused_computation.1 | convolution fusion | flops 939524096 | bytes 6225920 | tf_op jit(solution)/shard_map/dot_general | solution.py:458
  63.0 0.4 copy-done.3
  63.4 0.1 copy-done.5
  63.5 2.4 %add_convert_fusion = bf16[448,2048]{1,0:T(8,128)(2,1)} fusion(f32[448,2048]{1,0:T(8,128)S(1)} %fusion, bf16[448,512]{1,0:T(8,128)(2,1)S(1)} %copy-done.5, bf16[1,2048,512]{2,1,0:T(8,128)(2,1)S(1)} %copy-done.3), kind=kOutput, calls=%fused_computation | convolution fusion | flops 941359104 | bytes 8060928 | tf_op jit(solution)/shard_map/dot_general | solution.py:459
  65.9 0.1 reshape.34
  66.0 0.6 pad.4.gate_ref
  66.6 31.8 %combine.1 = (bf16[128,2048]{1,0:T(8,128)(2,1)}, f32[8,512]{1,0:T(8,128)}, f32[1,512]{1,0:T(1,128)}, f32[2,1,2048]{2,1,0:T(1,128)}) custom-call(bf16[8,56,2048]{2,1,0:T(8,128)(2,1)} %bitcast.35, f32[8,1,128]{2,1,0:T(1,128)} %pad.4.gate_ref, f32[2,1,2048]{2,1,0:T(1,128)} %get-tuple-element.26.rowsq_ref, bf16[128,2048]{1,0:T(8,128)(2,1)} %tok_ref.3, ...), custom_call_target="tpu_custom_call" | custom-call | tf_op jit(solution)/shard_map/combine/pallas_call | solution.py:546
  98.4 1.3 %slice_bitcast_fusion = (f32[1,2048]{1,0:T(1,128)}, f32[1,2048]{1,0:T(1,128)}) fusion(f32[2,1,2048]{2,1,0:T(1,128)} %get-tuple-element.35), kind=kLoop, calls=%fused_computation.15 | loop fusion | bytes 32768 | tf_op jit(solution)/shard_map/squeeze | solution.py:593
  99.7 1.9 %copy.20 = bf16[128,2048]{1,0:T(8,128)(2,1)} copy(bf16[128,2048]{1,0:T(8,128)(2,1)} %get-tuple-element.54) | data formatting | bytes 1048576
  101.6 1.3 %copy.21 = f32[512,8]{0,1:T(8,128)} copy(f32[512,8]{0,1:T(8,128)} %bitcast.44) | data formatting | bytes 32768
  103.0 1.2 %copy.22 = f32[512]{0:T(512)} copy(f32[512]{0:T(512)} %bitcast.47) | data formatting | bytes 4096
  (1 shorter events, 0.0 us)
Async XLA Ops:
  0.6 40.1 %copy-start = (bf16[1,2048,512]{2,1,0:T(8,128)(2,1)S(1)}, bf16[1,2048,512]{2,1,0:T(8,128)(2,1)}, u32[]{:S(2)}) copy-start(bf16[1,2048,512]{2,1,0:T(8,128)(2,1)} %param.10) | copy-start | bytes 6291460
  40.8 2.8 %copy-start.2 = (bf16[1,2048,512]{2,1,0:T(8,128)(2,1)S(1)}, bf16[1,2048,512]{2,1,0:T(8,128)(2,1)}, u32[]{:S(2)}) copy-start(bf16[1,2048,512]{2,1,0:T(8,128)(2,1)} %param.11) | copy-start | bytes 6291460
  40.8 2.8 %copy-start.4 = (bf16[8,56,2048]{2,1,0:T(8,128)(2,1)S(1)}, bf16[8,56,2048]{2,1,0:T(8,128)(2,1)}, u32[]{:S(2)}) copy-start(bf16[8,56,2048]{2,1,0:T(8,128)(2,1)} %get-tuple-element.25) | copy-start | bytes 5505028
  43.6 2.0 %copy-start.6 = (f32[8,1,128]{2,1,0:T(1,128)S(1)}, f32[8,1,128]{2,1,0:T(1,128)}, u32[]{:S(2)}) copy-start(f32[8,1,128]{2,1,0:T(1,128)} %get-tuple-element.23) | copy-start | bytes 12292
  51.5 10.3 %copy-start.1 = (bf16[448,512]{1,0:T(8,128)(2,1)S(1)}, bf16[448,512]{1,0:T(8,128)(2,1)}, u32[]{:S(2)}) copy-start(bf16[448,512]{1,0:T(8,128)(2,1)} %get-tuple-element.39.gate_ref) | copy-start | bytes 1376260
  61.8 1.6 %copy-start.3 = (bf16[1,2048,512]{2,1,0:T(8,128)(2,1)S(1)}, bf16[1,2048,512]{2,1,0:T(8,128)(2,1)}, u32[]{:S(2)}) copy-start(bf16[1,2048,512]{2,1,0:T(8,128)(2,1)} %param.11) | copy-start | bytes 6291460
  61.8 1.6 %copy-start.5 = (bf16[448,512]{1,0:T(8,128)(2,1)S(1)}, bf16[448,512]{1,0:T(8,128)(2,1)}, u32[]{:S(2)}) copy-start(bf16[448,512]{1,0:T(8,128)(2,1)} %get-tuple-element.40.up_ref) | copy-start | bytes 1376260

commit v3 on v2

--- a/solution.py
+++ b/solution.py
@@ -42,9 +42,18 @@
     return jnp.sum(jnp.where(ids == index, value, 0.0), axis=1, keepdims=True)
 
 
+def lane_sum(value):
+    total = value[:, :LANES]
+    for at in range(LANES, value.shape[1], LANES):
+        total = total + value[:, at : at + LANES]
+    return total
+
+
 def dispatch_kernel(
-    dims, tok_ref, cot_ref, routing_ref, router_ref,
-    rows_ref, cots_ref, scale_ref, aff_ref, pos_ref,
+    dims, tok_ref, cot_ref, routing_ref, router_ref, w_gate, w_up, w_down,
+    rows_out, cots_out, aff_ref, pos_ref, hidden_ref, gate_pre_ref, up_pre_ref, part_ref, term_ref,
+    column_ref,
+    rows_ref, cots_ref, scale_ref, gate_v, up_v, down_v, w_sem, flush_sem,
     stage, scale_stage, own_sem, sc_send, sc_recv, a_send, a_recv, y_send, y_recv, p_send, p_recv,
 ):
     n_ep, n_tp, n_batch, capacity, cap_pad, col_width = dims
@@ -57,6 +66,14 @@
     experts = router_ref.shape[0]
     tok_count = tok_ref.shape[0]
     outs = (rows_ref, cots_ref)
+    results = (rows_out, cots_out)
+    weight_copies = [
+        pltpu.make_async_copy(src.at[0], dst, w_sem.at[n])
+        for n, (src, dst) in enumerate(((w_gate, gate_v), (w_up, up_v), (w_down, down_v)))
+    ]
+    for copy in weight_copies:
+        copy.start()
+    term_ref[...] = jnp.zeros_like(term_ref)
 
     def cols(index):
         return pl.ds(pl.multiple_of(index * col_width, LANES), col_width)
@@ -128,54 +145,105 @@
                 p_copy(a, batch, y_from).start()
 
     my_batch = me // per
-    batches = [lax.rem(my_batch - i + n_batch, n_batch) for i in range(n_batch)]
-    for i, batch in enumerate(batches):
+
+    def batch_at(i):
+        return lax.rem(my_batch - i + 2 * n_batch, n_batch)
+
+    def flush(a, batch):
+        part = pl.ds(batch * per, per)
+        return pltpu.make_async_copy(outs[a].at[part], results[a].at[part], flush_sem.at[a, batch])
+
+    def arrive(batch):
         for a in range(2):
             for j in range(per):
                 source = batch * per + j
 
-                def from_other(a=a, source=source):
+                @pl.when(source == me)
+                def _(a=a, source=source):
+                    pltpu.make_async_copy(
+                        stage.at[a, source], outs[a].at[source, :, cols(tp)], own_sem.at[a]
+                    ).wait()
+
+                @pl.when(source != me)
+                def _(a=a, source=source):
                     ref = outs[a].at[source, :, cols(tp)]
                     remote(
                         ref, ref, a_send.at[a, source], a_recv.at[a, source], {"ep": source}
                     ).wait_recv()
 
-                def from_self(a=a, source=source):
-                    pltpu.make_async_copy(
-                        stage.at[a, source], outs[a].at[source, :, cols(tp)], own_sem.at[a]
-                    ).wait()
-
-                if per == 1:
-                    (from_self if i == 0 else from_other)()
-                elif i > 0:
-                    from_other()
-                else:
-                    pl.when(source == me)(from_self)
-                    pl.when(source != me)(from_other)
             for j in range(1, n_y):
                 y_copy(a, batch, lax.rem(y_at + j, n_y)).start()
             p_copy(a, batch, y_at).start()
-        if i > 1:
-            relay(batches[i - 2])
-    for batch in batches[-2:]:
-        relay(batch)
-    for batch in batches:
-        for a in range(2):
-            for j in range(n_y):
-                p_arrival(a, batch, lax.rem(y_at + j, n_y)).wait_recv()
+
+    def compute(source):
+        @pl.when(source == me)
+        def _():
+            pltpu.make_async_copy(scale_stage.at[source], scale_ref.at[source], own_sem.at[2]).wait()
+
+        @pl.when(source != me)
+        def _():
+            ref = scale_ref.at[source]
+            remote(ref, ref, sc_send.at[source], sc_recv.at[source], {"ep": source}).wait_recv()
+
+        scale = jnp.broadcast_to(scale_ref[source], (8, cap_pad)).T[:capacity, 0:1]
+        column_ref[source] = scale
+        rows_in, cots_in = rows_ref[source], cots_ref[source]
+        pre_gate = jnp.dot(rows_in, gate_v[...], preferred_element_type=F32)
+        pre_up = jnp.dot(rows_in, up_v[...], preferred_element_type=F32)
+        back = lax.dot_general(cots_in, down_v[...], COLS_T, preferred_element_type=F32)
+        sig = jax.nn.sigmoid(pre_gate)
+        hidden = (pre_gate * sig * pre_up).astype(BF16)
+        hidden_ref[source] = hidden
+        terms = lane_sum(hidden.astype(F32) * back)
+        term_ref[source, :, :capacity] = jnp.sum(terms.T, axis=0, keepdims=True)
+        scaled = scale * back
+        grad_up = (scaled * pre_gate * sig).astype(BF16)
+        grad_gate = (scaled * pre_up * sig * (1.0 + pre_gate * (1.0 - sig))).astype(BF16)
+        up_pre_ref[source] = grad_up
+        gate_pre_ref[source] = grad_gate
+        part = lax.dot_general(grad_gate, gate_v[...], COLS_T, preferred_element_type=F32)
+        part = part + lax.dot_general(grad_up, up_v[...], COLS_T, preferred_element_type=F32)
+        part_ref[source] = part.astype(BF16)
+
+    for copy in weight_copies:
+        copy.wait()
+
+    def step(i, carry):
+        @pl.when(i < n_batch)
+        def _():
+            arrive(batch_at(i))
+
+        @pl.when((i >= 1) & (i < n_batch + 1))
+        def _():
+            relay(batch_at(i - 1))
+
+        @pl.when(i >= 2)
+        def _():
+            batch = batch_at(i - 2)
+            for a in range(2):
+                for j in range(n_y):
+                    p_arrival(a, batch, lax.rem(y_at + j, n_y)).wait_recv()
+                flush(a, batch).start()
+            for j in range(per):
+                compute(batch * per + j)
+
+        return carry
+
+    lax.fori_loop(0, n_batch + 2, step, 0)
+    batches = range(n_batch)
     for i in range(1, n_ep):
         other = lax.rem(me + i, n_ep)
         remote(
             scale_stage.at[other], scale_ref.at[other], sc_send.at[other], sc_recv.at[other], {"ep": other}
-        ).wait()
+        ).wait_send()
         for a in range(2):
             remote(
                 stage.at[a, other], outs[a].at[me, :, cols(tp)], a_send.at[a, other],
                 a_recv.at[a, me], {"ep": other},
             ).wait_send()
-    pltpu.make_async_copy(scale_stage.at[me], scale_ref.at[me], own_sem.at[2]).wait()
     for batch in batches:
         for a in range(2):
+            flush(a, batch).wait()
             for j in range(n_y):
                 y_to = lax.rem(y_at + j, n_y)
                 if j > 0:
@@ -185,7 +253,7 @@
 
 def combine_kernel(
     dims, part_ref, gate_ref, rowsq_ref, tok_ref, routing_ref, router_ref, aff_ref, pos_ref,
-    token_ref, rgrad_ref, rrows_ref, rowsum_ref,
+    token_ref, rgrad_ref, rowsum_ref,
     r1, s1, r2, res, back, gate_in, gate_sum, gate_back, rowsq_in, rpart, rparts, tgrad,
     s1_send, s1_recv, s2_send, s2_recv, s3_send, s3_recv, gt_send, gt_recv, gb_send, gb_recv,
     rs_send, rs_recv, rp_send, rp_recv, ty_send, ty_recv, tp_send, tp_recv, own_sem,
@@ -372,7 +440,6 @@
         router_copy(source, source).wait_recv()
         rgrad = rgrad + rparts[source]
     rgrad_ref[...] = rgrad
-    rrows_ref[...] = jnp.sum(rgrad * rgrad, axis=0, keepdims=True)
     sums = rowsq_ref[...]
     for i in range(1, n_tp):
         other = lax.rem(tp + i, n_tp)
@@ -409,14 +476,6 @@
                 second(batch, y_to, y_at).wait_send()
 
 
-def lane_squares(value):
-    squares = value * value
-    total = squares[:, :LANES]
-    for at in range(LANES, value.shape[1], LANES):
-        total = total + squares[:, at : at + LANES]
-    return total
-
-
 def weight_grad_kernel(
     rows_ref, cots_ref, hidden_ref, gate_ref, up_ref, scale_ref,
     gate_out, up_out, down_out, squares_out, down_squares_out, hidden_t, down_acc,
@@ -432,34 +491,24 @@
     for a, (pre, out) in enumerate(((gate_ref, gate_out), (up_ref, up_out))):
         grad = jnp.dot(rows_t, pre[...], preferred_element_type=F32)
         out[...] = grad.astype(BF16)
-        squares_out[a] = jnp.sum(lane_squares(grad).T, axis=0, keepdims=True)
+        squares_out[a] = jnp.sum(lane_sum(grad * grad).T, axis=0, keepdims=True)
     weighted = (scale_ref[...] * cots_ref[...].astype(F32)).astype(BF16)
     grad = jnp.dot(hidden_t[...], weighted, preferred_element_type=F32)
     down_out[...] = grad.astype(BF16)
-    down_acc[...] += lane_squares(grad)
+    down_acc[...] += lane_sum(grad * grad)
 
     @pl.when(step == pl.num_programs(0) - 1)
     def _():
         down_squares_out[...] = jnp.sum(down_acc[...].T, axis=0, keepdims=True)
 
 
-def expert_backward(rows_in, cots_in, slot_scale, w_gate, w_up, w_down):
-    pre_gate = jnp.dot(rows_in, w_gate, preferred_element_type=F32)
-    pre_up = jnp.dot(rows_in, w_up, preferred_element_type=F32)
-    sigmoid_gate = jax.nn.sigmoid(pre_gate)
-    hidden = (pre_gate * sigmoid_gate * pre_up).astype(BF16)
-    back_proj = lax.dot_general(cots_in, w_down, COLS_T, preferred_element_type=F32)
-    gate_term = jnp.sum(hidden.astype(F32) * back_proj, axis=1)
-    scaled = slot_scale * back_proj
-    grad_up_pre = (scaled * pre_gate * sigmoid_gate).astype(BF16)
-    grad_gate_pre = (
-        scaled * pre_up * sigmoid_gate * (1.0 + pre_gate * (1.0 - sigmoid_gate))
-    ).astype(BF16)
-    partial_value = lax.dot_general(grad_gate_pre, w_gate, COLS_T, preferred_element_type=F32)
-    partial_value = partial_value + lax.dot_general(
-        grad_up_pre, w_up, COLS_T, preferred_element_type=F32
-    )
-    return partial_value.astype(BF16), gate_term, hidden, grad_gate_pre, grad_up_pre
+def finish_kernel(token_ref, router_ref, sums_ref, token_out, router_out, rows_out, gate_out, up_out):
+    token_out[...] = token_ref[...]
+    grad = router_ref[...]
+    router_out[...] = grad
+    rows_out[...] = jnp.sum(grad * grad, axis=0, keepdims=True)
+    gate_out[...] = sums_ref[0]
+    up_out[...] = sums_ref[1]
 
 
 def per_device(tokens, routing, router_weight, gate_weight, up_weight, down_weight, cotangent):
@@ -479,18 +528,36 @@
     hbm = pl.BlockSpec(memory_space=pl.ANY)
     dma = pltpu.SemaphoreType.DMA
 
-    rows, cots, scale, aff, pos = pl.pallas_call(
+    units = gate_weight.shape[2]
+
+    def per_slot(size, dtype):
+        return jax.ShapeDtypeStruct((n_ep, capacity, size), dtype)
+
+    (rows, cots, aff, pos, hidden, grad_gate_pre, grad_up_pre, partial_value, gate_term,
+     slot_scale) = pl.pallas_call(
         functools.partial(dispatch_kernel, dims),
         out_shape=(
-            jax.ShapeDtypeStruct((n_ep, capacity, width), BF16),
-            jax.ShapeDtypeStruct((n_ep, capacity, width), BF16),
-            jax.ShapeDtypeStruct((n_ep, 1, cap_pad), F32),
+            per_slot(width, BF16),
+            per_slot(width, BF16),
             jax.ShapeDtypeStruct((tok_count, experts), F32),
             jax.ShapeDtypeStruct((tok_count, experts), F32),
+            per_slot(units, BF16),
+            per_slot(units, BF16),
+            per_slot(units, BF16),
+            per_slot(width, BF16),
+            jax.ShapeDtypeStruct((n_ep, 1, cap_pad), F32),
+            per_slot(1, F32),
         ),
-        in_specs=[vmem] * 4,
-        out_specs=(hbm, hbm, vmem, vmem, vmem),
+        in_specs=[vmem] * 4 + [hbm] * 3,
+        out_specs=(hbm, hbm) + (vmem,) * 8,
         scratch_shapes=[
+            pltpu.VMEM((n_ep, capacity, width), BF16),
+            pltpu.VMEM((n_ep, capacity, width), BF16),
+            pltpu.VMEM((n_ep, 1, cap_pad), F32),
+            pltpu.VMEM((width, units), BF16),
+            pltpu.VMEM((width, units), BF16),
+            pltpu.VMEM((units, width), BF16),
+            dma((3,)), dma((2, n_batch)),
             pltpu.VMEM((2, n_ep, capacity, col_width), BF16),
             pltpu.VMEM((n_ep, 1, cap_pad), F32),
             dma((3,)),
@@ -501,19 +568,13 @@
         ],
         compiler_params=pltpu.CompilerParams(collective_id=0, has_side_effects=True),
         name="dispatch",
-    )(tokens, cotangent, routing.T, router_weight.T)
-
-    slot_scale = scale[:, 0, :capacity].reshape(slots)[:, None]
-    rows, cots = rows.reshape(slots, width), cots.reshape(slots, width)
-    partial_value, gate_term, hidden, grad_gate_pre, grad_up_pre = expert_backward(
-        rows, cots, slot_scale,
-        gate_weight[0], up_weight[0], down_weight[0],
-    )
-    gate_term = jnp.pad(
-        gate_term.reshape(n_ep, 1, capacity), ((0, 0), (0, 0), (0, cap_pad - capacity))
+    )(tokens, cotangent, routing.T, router_weight.T, gate_weight, up_weight, down_weight)
+
+    rows, cots, hidden, grad_gate_pre, grad_up_pre, slot_scale = (
+        value.reshape(slots, -1)
+        for value in (rows, cots, hidden, grad_gate_pre, grad_up_pre, slot_scale)
     )
     span = 2 * LANES if width % (2 * LANES) == 0 else LANES
-    units = hidden.shape[1]
     whole = pl.BlockSpec((slots, units), lambda i: (0, 0))
     grad_gate, grad_up, grad_down, row_squares, down_rows = pl.pallas_call(
         weight_grad_kernel,
@@ -543,16 +604,15 @@
         name="weight_grads",
     )(rows, cots, hidden, grad_gate_pre, grad_up_pre, slot_scale)
 
-    token_grad, router_grad, router_rows, row_sums = pl.pallas_call(
+    token_grad, router_grad, row_sums = pl.pallas_call(
         functools.partial(combine_kernel, dims),
         out_shape=(
             jax.ShapeDtypeStruct((tok_count, width), BF16),
             jax.ShapeDtypeStruct((experts, col_width), F32),
-            jax.ShapeDtypeStruct((1, col_width), F32),
             jax.ShapeDtypeStruct(row_squares.shape, F32),
         ),
         in_specs=[vmem] * 8,
-        out_specs=(hbm, vmem, vmem, vmem),
+        out_specs=(hbm, vmem, vmem),
         scratch_shapes=[
             pltpu.VMEM((n_y, n_ep, capacity, col_width), BF16),
             pltpu.VMEM((n_y, n_ep, capacity, col_width), BF16),
@@ -579,9 +639,22 @@
         ],
         compiler_params=pltpu.CompilerParams(collective_id=1, has_side_effects=True),
         name="combine",
-    )(partial_value.reshape(n_ep, capacity, width), gate_term, row_squares, tokens,
+    )(partial_value, gate_term, row_squares, tokens,
       routing.T, router_weight.T, aff, pos)
 
+    token_grad, router_grad, router_rows, gate_rows, up_rows = pl.pallas_call(
+        finish_kernel,
+        out_shape=(
+            jax.ShapeDtypeStruct((tok_count, width), BF16),
+            jax.ShapeDtypeStruct((experts, col_width), F32),
+            jax.ShapeDtypeStruct((1, col_width), F32),
+            jax.ShapeDtypeStruct((1, width), F32),
+            jax.ShapeDtypeStruct((1, width), F32),
+        ),
+        in_specs=[vmem] * 3,
+        out_specs=(vmem,) * 5,
+        name="finish",
+    )(token_grad, router_grad, row_sums)
     return (
         token_grad,
         router_grad.T,
@@ -589,8 +662,8 @@
         grad_gate[None],
         grad_up[None],
         grad_down[None],
-        row_sums[0],
-        row_sums[1],
+        gate_rows,
+        up_rows,
         down_rows,
     )
 

time: 106 us -> 98.8 us (0.932)
  Pallas kernels: 82.2 us -> 96.5 us
  matrix products: 13.4 us -> 0 us
  local copies, waits for them, and re-layouts: 7.84 us -> 0 us
    dot_general x5 -> x0, matrix products: 13.4 us -> none  [the longest x1 5 us: expert_backward(): lax.dot_general(cots_in, w_down, COLS_T, preferred_element_type=F32)]
    pallas_call x1 -> x2, Pallas kernels: 40.1 us -> 51.9 us  [the longest x1 50 us: per_device(): pl.pallas_call(functools.partial(dispatch_kernel, dims), out_shape=(per_s...]
    unnamed x17 -> x0, local copies, waits for them, and re-layouts: 4.92 us -> none
    pallas_call x1, Pallas kernels: 31.8 us -> 34.4 us  [per_device(): pl.pallas_call(functools.partial(combine_kernel, dims), out_shape=(jax.Sh...]
    squeeze x1 -> x0, local copies, waits for them, and re-layouts: 1.32 us -> none  [per_device(): row_sums[1]]
where the time goes in v3:
time: 98.8 us; the launch traced here: 97.2 us
  Pallas kernels  96.5 us (98%)
    pallas_call x1, Pallas kernels, per_device(): pl.pallas_call(functools.partial(dispatch_kernel, dims), out_shape=(per_s...  50 us
    pallas_call x1, Pallas kernels, per_device(): pl.pallas_call(functools.partial(combine_kernel, dims), out_shape=(jax.Sh...  34.4 us
    pallas_call x1, Pallas kernels, per_device(): pl.pallas_call(weight_grad_kernel, grid=(width // span,), out_shape=(jax....  10.3 us

profile of v3, /device:TPU:0, one launch (start us, length us, event | category | flops | bytes accessed | tf_op | source)
XLA Modules:
  0.0 97.2 jit_solution(5025842412385463682)
XLA Ops:
  0.6 50.0 %dispatch.1 = (bf16[8,56,2048]{2,1,0:T(8,128)(2,1)}, bf16[8,56,2048]{2,1,0:T(8,128)(2,1)}, f32[128,8]{1,0:T(8,128)}, f32[128,8]{1,0:T(8,128)}, bf16[8,56,512]{2,...) custom-call(bf16[128,2048]{1,0:T(8,128)(2,1)} %tok_ref.3, ...), custom_call_target="tpu_custom_call" | custom-call | tf_op jit(solution)/shard_map/dispatch/pallas_call | solution.py:537
  50.6 10.3 %weight_grads.1 = (bf16[2048,512]{1,0:T(8,128)(2,1)}, bf16[2048,512]{1,0:T(8,128)(2,1)}, bf16[512,2048]{1,0:T(8,128)(2,1)}, f32[2,1,2048]{2,1,0:T(1,128)}, f32[1,512]{1,0:T(1,128)}) custom-call(bf16[448,2048]{1,0:T(8,128)(2,1)} %bitcast.13, bf16[448,2048]{1,0:T(8,128)(2,1)} %bitcast.14, bf16[448,512]{1,0:T(8,128)(2,1)} %bitcast.15, ...), custom_call_target="tpu_custom_call" | custom-call | tf_op jit(solution)/shard_map/weight_grads/pallas_call | solution.py:579
  60.9 34.4 %combine.1 = (bf16[128,2048]{1,0:T(8,128)(2,1)}, f32[8,512]{1,0:T(8,128)}, f32[2,1,2048]{2,1,0:T(1,128)}) custom-call(bf16[8,56,2048]{2,1,0:T(8,128)(2,1)} %get-tuple-element.32.part_ref, f32[8,1,128]{2,1,0:T(1,128)} %get-tuple-element.33.gate_ref, f32[2,1,2048]{2,1,0:T(1,128)} %get-tuple-element.40.rowsq_ref, bf16[128,2048]{1,0:T(8,128)(2,1)} %tok_ref.3, ...), custom_call_target="tpu_custom_call" | custom-call | tf_op jit(solution)/shard_map/combine/pallas_call | solution.py:607
  95.3 1.9 %finish.1 = (bf16[128,2048]{1,0:T(8,128)(2,1)}, f32[8,512]{1,0:T(8,128)}, f32[1,512]{1,0:T(1,128)}, f32[1,2048]{1,0:T(1,128)}, f32[1,2048]{1,0:T(1,128)}) custom-call(bf16[128,2048]{1,0:T(8,128)(2,1)} %get-tuple-element.43.token_ref, f32[8,512]{1,0:T(8,128)} %get-tuple-element.44.router_ref, f32[2,1,2048]{2,1,0:T(1,128)} %get-tuple-element.45.sums_ref), custom_call_target="tpu_custom_call" | custom-call | tf_op jit(solution)/shard_map/finish/pallas_call | solution.py:645
